TPU v7x, 32 devices: a whole 2x2x4 slice. The times are simulated.
32 devices in a mesh: rep: 2 (over x), fs: 8 (over z, y), tp: 2 (over core).
Axes of the slice: x: 2, y: 2, z: 4, core: 2. Of those that a mesh axis runs over, the one named last changes fastest.
Arguments:
- pre_gate: bfloat16 [12288, 4096], P(('rep', 'fs'), 'tp'), may hold values from -6 to 6
- pre_linear: bfloat16 [12288, 4096], P(('rep', 'fs'), 'tp'), may hold values from -6 to 6
- taps_gate: float32 [3, 4096], P(None, 'tp'), may hold values from -3.5 to 3.5
- taps_linear: float32 [3, 4096], P(None, 'tp'), may hold values from -3.5 to 3.5
- bias_gate: float32 [4096], P('tp'), may hold values from -3 to 3
- bias_linear: float32 [4096], P('tp'), may hold values from -3 to 3
- down_weight: bfloat16 [4096, 2048], P('tp', 'fs'), may hold values from -0.09375 to 0.09375
- out_grad: bfloat16 [12288, 2048], P(('rep', 'fs')), may hold values from -8 to 8
Outputs:
- grad_gate: bfloat16 [12288, 4096], P(('rep', 'fs'), 'tp')
- grad_linear: bfloat16 [12288, 4096], P(('rep', 'fs'), 'tp')
- grad_taps_gate: float32 [3, 4096], P(None, 'tp')
- grad_taps_linear: float32 [3, 4096], P(None, 'tp')
- grad_bias_gate: float32 [4096], P('tp')
- grad_bias_linear: float32 [4096], P('tp')
- grad_down: float32 [4096, 2048], P('tp', 'fs')
- row_norms: float32 [4096], P('tp')
All inputs are finite; a program needn't handle non-finite values.
Results may differ from a plain program's by a relative error of at most 0.0031.
Values may be sent and summed in bfloat16 or wider, within the bound.
No kernel may reach another device: no remote copies, remote signals or barrier semaphores. Data moves between devices by JAX's collectives and lax.ppermute only.
A program may use at most 128 MiB of HBM per device.

v0:
```python
import functools

import jax
import jax.numpy as jnp
from jax import lax
from jax.experimental import pallas as pl
from jax.experimental.pallas import tpu as pltpu
from jax.sharding import PartitionSpec as P


HALVES = 2
GATE_CALLS = 2
F32, BF16 = jnp.float32, jnp.bfloat16


RING = 4


def swap(value, axis, size, distance):
    return lax.ppermute(value, axis, [(i, i ^ distance) for i in range(size)])


def ring(value, size, steps):
    inner = size // RING
    pairs = [(i, (i // inner + steps) % RING * inner + i % inner) for i in range(size)]
    return lax.ppermute(value, "fs", pairs)


def bits_below(size):
    return [1 << k for k in range(size.bit_length() - 1)]


def pair_sum(value, axis, size, distances):
    got = [swap(value, axis, size, d) for d in distances]
    if len(distances) == 1:
        return value + got[0]
    third = swap(value, axis, size, distances[0] ^ distances[1])
    return (value + got[0]) + (got[1] + third)


def lane_block(length):
    return min(length, 256)


def row_step(length):
    return 64 if length % 64 == 0 else 32 if length % 32 == 0 else 16


def hidden_kernel(block_rows, at_ref, gate_ref, linear_ref, tg_ref, tl_ref, bg_ref, bl_ref, out_ref, made):
    rows, lanes = gate_ref.shape
    step = row_step(block_rows)
    flip = at_ref[1]

    def convolved(ref, taps_ref, bias_ref, start, cols):
        now = ref[pl.ds(start, step), cols].astype(F32)
        back = pl.multiple_of(jnp.maximum(start - 16, 0), 16)
        halo = ref[pl.ds(back, 16), cols].astype(F32)[8:16]
        halo = jnp.where(start > 0, halo, 0.0)
        ext = jnp.concatenate([halo, now], 0)
        one, two = pltpu.roll(ext, 1, 0)[8:], pltpu.roll(ext, 2, 0)[8:]
        return (
            taps_ref[0:1, cols] * two
            + taps_ref[1:2, cols] * one
            + taps_ref[2:3, cols] * now
            + bias_ref[0:1, cols]
        )

    for lane in range(0, lanes, 128):
        cols = slice(lane, lane + 128)

        def body(i, carry):
            start = pl.multiple_of(i * step, step)
            g = convolved(gate_ref, tg_ref, bg_ref, start, cols)
            l = convolved(linear_ref, tl_ref, bl_ref, start, cols)
            block, rest = start // block_rows, start % block_rows
            to = pl.multiple_of((block ^ flip) * block_rows + rest, 16)
            made[pl.ds(to, step), cols] = (g * jax.nn.sigmoid(g) * l).astype(BF16)
            return carry

        lax.fori_loop(0, rows // step, body, 0, unroll=2)
    out_ref[...] = made[...].T


def hidden_half(which, flip, block_rows, pre_gate, pre_linear, taps_gate, taps_linear, bias_gate, bias_linear):
    rows, width = pre_gate.shape
    half = width // 2
    lanes = lane_block(half)
    steps = half // lanes
    wide = pl.BlockSpec((rows, lanes), lambda i, at: (0, at[0] * steps + i))
    taps = pl.BlockSpec((3, lanes), lambda i, at: (0, at[0] * steps + i))
    bias = pl.BlockSpec((1, lanes), lambda i, at: (0, at[0] * steps + i))
    return pl.pallas_call(
        functools.partial(hidden_kernel, block_rows),
        grid_spec=pltpu.PrefetchScalarGridSpec(
            num_scalar_prefetch=1,
            grid=(steps,),
            in_specs=[wide, wide, taps, taps, bias, bias],
            out_specs=pl.BlockSpec((lanes, rows), lambda i, at: (i, 0)),
            scratch_shapes=[pltpu.VMEM((rows, lanes), BF16)],
        ),
        out_shape=jax.ShapeDtypeStruct((half, rows), BF16),
        cost_estimate=pl.CostEstimate(
            flops=3000 * rows * half, bytes_accessed=6 * rows * half, transcendentals=rows * half
        ),
        name="hidden",
        compiler_params=pltpu.CompilerParams(vmem_limit_bytes=12 << 20),
    )(
        jnp.stack([which, flip]).astype(jnp.int32),
        pre_gate,
        pre_linear,
        taps_gate,
        taps_linear,
        bias_gate[None],
        bias_linear[None],
    )


def column_block(tokens, cols, index):
    if tokens.ndim == 3:
        return pl.BlockSpec((None, *tokens.shape[1:]), lambda j, at: (index(j, at), 0, 0))
    return pl.BlockSpec((tokens.shape[0], cols), lambda j, at: (0, index(j, at)))


def own_kernel(at_ref, hidden_ref, tokens_ref, out_ref):
    out_ref[...] = lax.dot_general(
        hidden_ref[...], tokens_ref[...], (((1,), (0,)), ((), ())), preferred_element_type=F32
    )


def own_blocks(blocks, cols, hidden, tokens):
    half, rows = hidden.shape
    count = len(blocks)
    return pl.pallas_call(
        own_kernel,
        grid_spec=pltpu.PrefetchScalarGridSpec(
            num_scalar_prefetch=1,
            grid=(count,),
            in_specs=[
                pl.BlockSpec((half, rows), lambda j, at: (0, 0)),
                column_block(tokens, cols, lambda j, at: at[j]),
            ],
            out_specs=pl.BlockSpec((None, half, cols), lambda j, at: (j, 0, 0)),
        ),
        out_shape=jax.ShapeDtypeStruct((count, half, cols), F32),
        compiler_params=pltpu.CompilerParams(vmem_limit_bytes=24 << 20),
        cost_estimate=pl.CostEstimate(
            flops=2 * rows * half * cols * count, bytes_accessed=2 * rows * (half + cols * count), transcendentals=0
        ),
        name="own",
    )(jnp.stack(blocks).astype(jnp.int32), hidden, tokens)


def outer_kernel(groups, kind, n_tokens, at_ref, hidden_ref, before_ref, *refs):
    tokens, outs = refs[:n_tokens], refs[n_tokens:]
    right = jnp.concatenate([t[...] for t in tokens], 0)
    made = before_ref[...] + lax.dot_general(
        hidden_ref[...], right, (((1,), (0,)), ((), ())), preferred_element_type=F32
    )
    made = made.astype(kind)
    rows = made.shape[0] // HALVES
    at = 0
    for h, counts in enumerate(groups):
        step = 0
        for count in counts:
            for slot in range(count):

                @pl.when(pl.program_id(0) == step)
                def _(at=at, slot=slot, h=h):
                    outs[at][slot] = made[h * rows : (h + 1) * rows]

                step += 1
            at += 1


def outer_blocks(groups, kind, blocks, cols, hidden, shares, before, first):
    half, rows = hidden.shape
    count = len(blocks)
    shapes = [(c, half // HALVES, cols) for counts in groups for c in counts]
    outs = pl.pallas_call(
        functools.partial(outer_kernel, groups, kind, len(shares)),
        grid_spec=pltpu.PrefetchScalarGridSpec(
            num_scalar_prefetch=1,
            grid=(count,),
            in_specs=[
                pl.BlockSpec((half, rows), lambda j, at: (0, 0)),
                pl.BlockSpec((None, half, cols), lambda j, at: (first + j, 0, 0)),
                *[column_block(t, cols, lambda j, at: at[j]) for t in shares],
            ],
            out_specs=[pl.BlockSpec(s, lambda j, at: (0, 0, 0)) for s in shapes],
        ),
        out_shape=[jax.ShapeDtypeStruct(s, kind) for s in shapes],
        compiler_params=pltpu.CompilerParams(vmem_limit_bytes=24 << 20),
        cost_estimate=pl.CostEstimate(
            flops=2 * rows * half * cols * count, bytes_accessed=2 * rows * (half + cols * count), transcendentals=0
        ),
        name="outer",
    )(jnp.stack(blocks).astype(jnp.int32), hidden, before, *shares)
    result, at = [], 0
    for counts in groups:
        result.append(outs[at : at + len(counts)])
        at += len(counts)
    return result


def gate_kernel(size, aliased, at_ref, tokens_ref, *refs):
    weights = refs[:size]
    gate_ref, linear_ref, tg_ref, tl_ref, bg_ref, bl_ref = refs[size : size + 6]
    gate_out, linear_out, sums_out, grads = refs[size + 6 + 3 * aliased :]
    rows, lanes = gate_ref.shape
    step = row_step(rows)
    cols = weights[0].shape[1]

    def block(p):
        at = at_ref[p]
        if len(tokens_ref.shape) == 3:
            return tokens_ref[at]
        return tokens_ref[:, pl.ds(pl.multiple_of(at * cols, cols), cols)]

    grads[...] = lax.dot_general(
        jnp.concatenate([block(p) for p in range(size)], 1),
        jnp.concatenate([w[...] for w in weights], 1),
        (((1,), (1,)), ((), ())),
        preferred_element_type=F32,
    )
    count = rows // step

    def fold(x):
        return jnp.sum(x.reshape(step // 8, 8, 128), axis=0)

    for lane in range(0, lanes, 128):
        here = slice(lane, lane + 128)

        def taps_at(ref, start):
            now = ref[pl.ds(start, step), here].astype(F32)
            back = pl.multiple_of(jnp.maximum(start - 16, 0), 16)
            halo = ref[pl.ds(back, 16), here].astype(F32)[8:16]
            halo = jnp.where(start > 0, halo, 0.0)
            ext = jnp.concatenate([halo, now], 0)
            return pltpu.roll(ext, 2, 0)[8:], pltpu.roll(ext, 1, 0)[8:], now

        def back(new, later, taps_ref):
            ext = jnp.concatenate([new, later], 0)
            one = pltpu.roll(ext, step + 7, 0)[:step]
            two = pltpu.roll(ext, step + 6, 0)[:step]
            return taps_ref[0:1, here] * two + taps_ref[1:2, here] * one + taps_ref[2:3, here] * new

        def body(i, carry):
            later_g, later_l, sums = carry
            start = pl.multiple_of((count - 1 - i) * step, step)
            g2, g1, g0 = taps_at(gate_ref, start)
            l2, l1, l0 = taps_at(linear_ref, start)
            gate_pre = tg_ref[0:1, here] * g2 + tg_ref[1:2, here] * g1 + tg_ref[2:3, here] * g0 + bg_ref[0:1, here]
            linear_pre = tl_ref[0:1, here] * l2 + tl_ref[1:2, here] * l1 + tl_ref[2:3, here] * l0 + bl_ref[0:1, here]
            sigma = jax.nn.sigmoid(gate_pre)
            grad = grads[pl.ds(start, step), here]
            d_gate = grad * linear_pre * sigma * (1.0 + gate_pre * (1.0 - sigma))
            d_linear = grad * (gate_pre * sigma)
            gate_out[pl.ds(start, step), here] = back(d_gate, later_g, tg_ref).astype(BF16)
            linear_out[pl.ds(start, step), here] = back(d_linear, later_l, tl_ref).astype(BF16)
            terms = (d_gate * g2, d_gate * g1, d_gate * g0, d_linear * l2, d_linear * l1, d_linear * l0, d_gate, d_linear)
            return d_gate[:8], d_linear[:8], tuple(s + fold(t) for s, t in zip(sums, terms))

        zero = jnp.zeros((8, 128), F32)
        _, _, sums = lax.fori_loop(0, count, body, (zero, zero, (zero,) * 8))
        sums_out[:, here] = jnp.concatenate([jnp.sum(s, axis=0, keepdims=True) for s in sums], 0)


def gate_part(call, tokens, index, own, others, pre_gate, pre_linear, taps_gate, taps_linear, bias_gate, bias_linear, before):
    rows, width = pre_gate.shape
    parts = HALVES * GATE_CALLS
    count = width // parts
    lanes = lane_block(count)
    steps = count // lanes
    cols = own.shape[1]
    inner = call % GATE_CALLS
    at = lambda i, s: (0, call * steps + i)
    wide = pl.BlockSpec((rows, lanes), at)
    aliased = before is not None
    extra = list(before) if aliased else []
    size = 1 + len(others)
    if tokens.ndim == 3:
        whole = pl.BlockSpec(tokens.shape, lambda i, s: (0, 0, 0))
    else:
        whole = pl.BlockSpec(tokens.shape, lambda i, s: (0, 0))
    return pl.pallas_call(
        functools.partial(gate_kernel, size, aliased),
        grid_spec=pltpu.PrefetchScalarGridSpec(
            num_scalar_prefetch=1,
            grid=(steps,),
            in_specs=[
                whole,
                pl.BlockSpec((lanes, cols), lambda i, s: (call * steps + i, 0)),
                *[pl.BlockSpec((lanes, cols), lambda i, s: (inner * steps + i, 0)) for _ in others],
                wide,
                wide,
                pl.BlockSpec((3, lanes), at),
                pl.BlockSpec((3, lanes), at),
                pl.BlockSpec((1, lanes), at),
                pl.BlockSpec((1, lanes), at),
                *[pl.BlockSpec(memory_space=pl.ANY) for _ in extra],
            ],
            out_specs=[wide, wide, pl.BlockSpec((8, lanes), at)],
            scratch_shapes=[pltpu.VMEM((rows, lanes), F32)],
        ),
        out_shape=[
            jax.ShapeDtypeStruct(pre_gate.shape, BF16),
            jax.ShapeDtypeStruct(pre_gate.shape, BF16),
            jax.ShapeDtypeStruct((8, width), F32),
        ],
        input_output_aliases={8 + size + j: j for j in range(len(extra))},
        cost_estimate=pl.CostEstimate(
            flops=5000 * rows * count, bytes_accessed=8 * rows * count, transcendentals=rows * count
        ),
        name="gate",
        compiler_params=pltpu.CompilerParams(vmem_limit_bytes=20 << 20),
    )(
        index,
        tokens,
        own,
        *others,
        pre_gate,
        pre_linear,
        taps_gate,
        taps_linear,
        bias_gate[None],
        bias_linear[None],
        *extra,
    )


def local(sizes, pre_gate, pre_linear, taps_gate, taps_linear, bias_gate, bias_linear, down_weight, out_grad):
    fs, tp = sizes["fs"], sizes["tp"]
    inner = fs // RING
    rep_at, fs_at, tp_at = (lax.axis_index(a) for a in ("rep", "fs", "tp"))
    out_at, in_at = fs_at // inner, fs_at % inner
    cols = out_grad.shape[1] // fs
    params = (pre_gate, pre_linear, taps_gate, taps_linear, bias_gate, bias_linear)

    def block_at(d, q):
        return (out_at + d) % RING * inner + (in_at ^ q)

    def blocked(tokens):
        if cols % 128 == 0:
            return tokens
        return tokens.reshape(tokens.shape[0], fs, cols).transpose(1, 0, 2)

    rows = out_grad.shape[0] // tp
    share = swap(lax.dynamic_slice_in_dim(out_grad, tp_at * rows, rows, 0), "rep", 2, 1)

    to_send = hidden_half(1 - rep_at, tp_at, rows, *params)
    arrived = swap(to_send, "rep", 2, 1)
    kept = hidden_half(rep_at, jnp.zeros_like(tp_at), rows, *params)

    w_rows = down_weight.shape[0] // HALVES
    late, _ = lax.optimization_barrier((down_weight, to_send))
    halves = [down_weight[:w_rows], late[w_rows:]]
    pieces = []
    for h in range(HALVES):
        have = {(0, 0): halves[h]}
        have[1, 0] = ring(have[0, 0], fs, 1)
        have[3, 0] = ring(have[0, 0], fs, -1)
        have[2, 0] = ring(have[1, 0], fs, 1)
        for q in range(1, inner):
            for d in (0, 1, 3, 2):
                if h and d == 2 and q == inner - 1:
                    have[d, q] = ring(have[1, q], fs, 1)
                else:
                    rest = q & (q - 1)
                    have[d, q] = swap(have[d, rest], "fs", fs, q ^ rest)
        pieces.append(have)

    shares = [share]
    for distance in bits_below(tp):
        shares = shares + [swap(v, "tp", tp, distance) for v in shares]
    shares = [blocked(t) for t in shares]
    tokens = blocked(out_grad)

    even = range(0, inner, 2)
    kept_places = [(d, q) for d in (2, 3, 1, 0) for q in even]
    held_blocks = [block_at(d, q) for d, q in kept_places]
    sent_blocks = [block_at(d, q ^ 1) for d, q in kept_places]
    count = len(even)
    groups = [[2 * count, 2 * count], [2 * count, count, count]]
    mine = own_blocks(sent_blocks + held_blocks, cols, kept, tokens)
    sent = outer_blocks(groups, BF16, sent_blocks, cols, arrived, shares, mine, 0)
    held = outer_blocks(groups, F32, held_blocks, cols, arrived, shares, mine, len(sent_blocks))
    finished = []
    for h in range(HALVES):
        sums = {}
        start = 0
        for keep, send in zip(held[h], sent[h]):
            both = keep + swap(send, "fs", fs, 1).astype(F32)
            sums.update({place: both[j] for j, place in enumerate(kept_places[start : start + both.shape[0]])})
            start += both.shape[0]
        for bit in bits_below(inner)[1:]:
            for d in range(RING):
                for q in even:
                    if q & -q == bit:
                        got = swap(sums[d, q].astype(BF16), "fs", fs, bit)
                        sums[d, q ^ bit] = sums[d, q ^ bit] + got.astype(F32)
        two = ring(sums[2, 0].astype(BF16), fs, 1)
        three = ring(sums[3, 0].astype(BF16), fs, -1)
        one = ring((sums[1, 0] + two.astype(F32)).astype(BF16), fs, 1)
        finished.append(sums[0, 0] + three.astype(F32) + one.astype(F32))
    theirs = [swap(v, "rep", 2, 1) for v in finished]
    first = rep_at == 0
    grad_down = jnp.concatenate(
        [jnp.where(first, v, w) for v, w in zip(finished, theirs)]
        + [jnp.where(first, w, v) for v, w in zip(finished, theirs)],
        0,
    )

    outs = None
    places = [(d, q) for q in range(inner) for d in (0, 1, 3, 2)]
    index = jnp.stack([block_at(-d, q) for d, q in places]).astype(jnp.int32)
    for call in range(HALVES * GATE_CALLS):
        others = [pieces[call // GATE_CALLS][place] for place in places[1:]]
        outs = gate_part(call, tokens, index, down_weight, others, *params, outs)
    grad_gate, grad_linear, packed = outs

    squares = jnp.concatenate([jnp.sum(v * v, axis=1) for v in finished])
    width = packed.shape[1]
    value = jnp.concatenate([packed, squares.reshape(8, -1)], 1)
    everyone = ("rep", "fs")
    spans = bits_below(fs)[::-1]
    pairs = len(spans) // 2
    for j in range(pairs):
        value = pair_sum(value, everyone, 2 * fs, spans[2 * j : 2 * j + 2])
    there = swap(value, everyone, 2 * fs, fs)
    for span in spans[2 * pairs :]:
        there = there + swap(value, everyone, 2 * fs, fs ^ span)
        value = value + swap(value, everyone, 2 * fs, span)
    packed = value[:, :width] + there[:, :width]
    norm, norm2 = value[:, width:].reshape(-1), there[:, width:].reshape(-1)
    row_norms = jnp.concatenate([jnp.where(first, norm, norm2), jnp.where(first, norm2, norm)], 0)
    return grad_gate, grad_linear, packed[0:3], packed[3:6], packed[6], packed[7], grad_down, row_norms


def solution(mesh):
    sizes = dict(mesh.shape)
    in_specs = (
        P(("rep", "fs"), "tp"),
        P(("rep", "fs"), "tp"),
        P(None, "tp"),
        P(None, "tp"),
        P("tp"),
        P("tp"),
        P("tp", "fs"),
        P(("rep", "fs"), None),
    )
    out_specs = (
        P(("rep", "fs"), "tp"),
        P(("rep", "fs"), "tp"),
        P(None, "tp"),
        P(None, "tp"),
        P("tp"),
        P("tp"),
        P("tp", "fs"),
        P("tp"),
    )

    def body(*args):
        return local(sizes, *args)

    return jax.shard_map(body, mesh=mesh, in_specs=in_specs, out_specs=out_specs, check_vma=False)
```

profile of v0, /device:TPU:0, one launch (start us, length us, event | category | flops | bytes accessed | tf_op | source)
XLA Modules:
  0.0 226.2 jit_solution(2629326151925469080)
XLA Ops:
  0.7 2.9 %constant_dynamic-slice_fusion = bf16[384,2048]{1,0:T(8,128)(2,1)} fusion(bf16[768,2048]{1,0:T(8,128)(2,1)} %tokens_ref.9, s32[]{:T(128)S(6)} %select_n.107), kind=kLoop, calls=%fused_computation.34 | loop fusion | bytes 3145732 | tf_op jit(solution)/shard_map/dynamic_slice | solution.py:348
  3.6 3.0 %collective-permute-start.15 = (bf16[384,2048]{1,0:T(8,128)(2,1)}, bf16[384,2048]{1,0:T(8,128)(2,1)}, u32[]{:S(2)}, u32[]{:S(2)}) collective-permute-start(bf16[384,2048]{1,0:T(8,128)(2,1)} %constant_dynamic-slice_fusion), channel_id=1, source_target_pairs={{0,16},{16,0},{1,17},{17,1},{2,18},{18,2},{3,19},{19,3},{4,20},{20... | collective-permute-start | bytes 4718600 | tf_op jit(solution)/shard_map/ppermute | solution.py:20
  6.5 1.9 slice.53
  8.4 1.6 collective-permute-start.7
  10.0 2.2 collective-permute-start.8
  12.2 1.5 collective-permute-start.10
  13.9 1.9 copy-done.6
  15.7 5.9 %hidden.2 = bf16[1024,768]{1,0:T(8,128)(2,1)} custom-call(s32[2]{0:T(128)S(1)} %pad_add_fusion.at_ref, bf16[768,2048]{1,0:T(8,128)(2,1)S(1)} %copy-done.3, bf16[768,2048]{1,0:T(8,128)(2,1)S(1)} %copy-done.6, f32[3,2048]{1,0:T(4,128)S(1)} %copy-done.11, f32[3,2048]{1,0:T(4,128)S(1)} %copy-done.12, f32[1,2048]{1,0:T(1,128)S(1)} %bitcast.59, f32[1,2048]{1,0:T(1,128)S(1)} %bitcast.65), custom_call_target="tpu_custom_call" | custom-call | flops 2359296000 | bytes 4718592 | tf_op jit(solution)/shard_map/hidden/pallas_call | solution.py:92
  22.2 19.9 %collective-permute-done.15.refs_0_ = bf16[384,2048]{1,0:T(8,128)(2,1)} collective-permute-done((bf16[384,2048]{1,0:T(8,128)(2,1)}, bf16[384,2048]{1,0:T(8,128)(2,1)}, u32[]{:S(2)}, u32[]{:S(2)}) %collective-permute-start.15) | collective-permute-done | bytes 1572896 | tf_op jit(solution)/shard_map/ppermute | solution.py:20
  42.9 2.1 collective-permute-start
  45.1 2.1 collective-permute-start.1
  47.1 13.1 %collective-permute-done.refs_1_ = bf16[1024,256]{1,0:T(8,128)(2,1)} collective-permute-done((bf16[1024,256]{1,0:T(8,128)(2,1)}, bf16[1024,256]{1,0:T(8,128)(2,1)}, u32[]{:S(2)}, u32[]{:S(2)}) %collective-permute-start) | collective-permute-done | bytes 524320 | tf_op jit(solution)/shard_map/ppermute | solution.py:26
  60.2 1.7 collective-permute-start.11
  62.0 8.6 %collective-permute-done.1.refs_2_ = bf16[1024,256]{1,0:T(8,128)(2,1)} collective-permute-done((bf16[1024,256]{1,0:T(8,128)(2,1)}, bf16[1024,256]{1,0:T(8,128)(2,1)}, u32[]{:S(2)}, u32[]{:S(2)}) %collective-permute-start.1) | collective-permute-done | bytes 524320 | tf_op jit(solution)/shard_map/ppermute | solution.py:26
  70.7 1.5 collective-permute-start.12
  72.2 10.3 %collective-permute-done.9.refs_3_ = bf16[1024,256]{1,0:T(8,128)(2,1)} collective-permute-done((bf16[1024,256]{1,0:T(8,128)(2,1)}, bf16[1024,256]{1,0:T(8,128)(2,1)}, u32[]{:S(2)}, u32[]{:S(2)}) %collective-permute-start.9) | collective-permute-done | bytes 524320 | tf_op jit(solution)/shard_map/ppermute | solution.py:26
  82.5 1.5 collective-permute-start.4
  84.2 1.9 copy-done.4
  86.1 1.9 copy-done.7
  88.0 5.1 %hidden.3.hidden_ref = bf16[1024,768]{1,0:T(8,128)(2,1)S(1)} custom-call(s32[2]{0:T(128)S(1)} %pad_add_fusion.2.at_ref, bf16[768,2048]{1,0:T(8,128)(2,1)S(1)} %copy-done.4, bf16[768,2048]{1,0:T(8,128)(2,1)S(1)} %copy-done.7, f32[3,2048]{1,0:T(4,128)S(1)} %copy-done.11, f32[3,2048]{1,0:T(4,128)S(1)} %copy-done.12, f32[1,2048]{1,0:T(1,128)S(1)} %bitcast.60, ...), custom_call_target="tpu_custom_call" | custom-call | flops 2359296000 | bytes 4718592 | tf_op jit(solution)/shard_map/hidden/pallas_call | solution.py:92
  93.7 5.7 %own.1.before_ref = f32[8,1024,256]{2,1,0:T(8,128)S(1)} custom-call(s32[8]{0:T(128)S(1)} %stack.98.at_ref, bf16[1024,768]{1,0:T(8,128)(2,1)S(1)} %hidden.3.hidden_ref, bf16[768,2048]{1,0:T(8,128)(2,1)S(1)} %copy-done), custom_call_target="tpu_custom_call" | custom-call | flops 3221225472 | bytes 4718592 | tf_op jit(solution)/shard_map/own/pallas_call | solution.py:133
  99.4 3.3 %copy-done.1 = f32[8,1024,256]{2,1,0:T(8,128)} copy-done((f32[8,1024,256]{2,1,0:T(8,128)}, f32[8,1024,256]{2,1,0:T(8,128)S(1)}, u32[]{:S(2)}) %copy-start.1) | copy-done | bytes 8388632
  102.7 1.5 collective-permute-start.3
  104.3 2.5 %collective-permute-start.2 = (bf16[1024,256]{1,0:T(8,128)(2,1)}, bf16[1024,256]{1,0:T(8,128)(2,1)}, u32[]{:S(2)}, u32[]{:S(2)}) collective-permute-start(bf16[1024,256]{1,0:T(8,128)(2,1)} %collective-permute-done.refs_1_), channel_id=1, source_target_pairs={{0,4},{2,6},{4,8},{6,10},{8,12},{10,14},{12,0},{14,2},{1,5},{3,7},... | collective-permute-start | bytes 1572872 | tf_op jit(solution)/shard_map/ppermute | solution.py:26
  108.1 2.1 collective-permute-start.6
  110.3 3.4 %copy-done.2 = f32[8,1024,256]{2,1,0:T(8,128)S(1)} copy-done((f32[8,1024,256]{2,1,0:T(8,128)S(1)}, f32[8,1024,256]{2,1,0:T(8,128)}, u32[]{:S(2)}) %copy-start.2) | copy-done | bytes 8388632
  113.7 5.5 %outer.3 = (bf16[2,512,256]{2,1,0:T(8,128)(2,1)S(1)}, bf16[2,512,256]{2,1,0:T(8,128)(2,1)S(1)}, bf16[2,512,256]{2,1,0:T(8,128)(2,1)S(1)}, bf16[1,512,256]{2,1,0:T(8,128)(2,1)S(1)}, bf16[1,512,256]{2,1,0:T(8,128)(2,1)S(1)}) custom-call(s32[4]{0:T(128)S(1)} %pad_add_fusion.3.at_ref, bf16[1024,768]{1,0:T(8,128)(2,1)} %collective-permute-done.14.hidden_ref, ...), custom_call_target="tpu_custom_call" | custom-call | flops 1610612736 | bytes 3145728 | tf_op jit(solution)/shard_map/outer/pallas_call | solution.py:179
  120.3 8.8 %gate.4 = (bf16[768,2048]{1,0:T(8,128)(2,1)}, bf16[768,2048]{1,0:T(8,128)(2,1)}, f32[8,2048]{1,0:T(8,128)S(1)}) custom-call(s32[8]{0:T(128)S(1)} %stack.87.at_ref, bf16[768,2048]{1,0:T(8,128)(2,1)S(1)} %copy-done, bf16[2048,256]{1,0:T(8,128)(2,1)S(1)} %copy-done.10, bf16[1024,256]{1,0:T(8,128)(2,1)} %collective-permute-done.7.refs_1_, ...), custom_call_target="tpu_custom_call" | custom-call | flops 1966080000 | bytes 3145728 | tf_op jit(solution)/shard_map/gate/pallas_call | solution.py:285
  129.1 8.8 %gate.5 = (bf16[768,2048]{1,0:T(8,128)(2,1)}, bf16[768,2048]{1,0:T(8,128)(2,1)}, f32[8,2048]{1,0:T(8,128)S(1)}) custom-call(s32[8]{0:T(128)S(1)} %stack.87.at_ref, bf16[768,2048]{1,0:T(8,128)(2,1)S(1)} %copy-done, bf16[2048,256]{1,0:T(8,128)(2,1)S(1)} %copy-done.10, ...), custom_call_target="tpu_custom_call", output_to_operand_aliasing={{0}: (16, {}), {1}: (17, {}), {2}: (18, {})} | custom-call | flops 1966080000 | bytes 3145728 | tf_op jit(solution)/shard_map/gate/pallas_call | solution.py:285
  138.0 9.1 %gate.6 = (bf16[768,2048]{1,0:T(8,128)(2,1)}, bf16[768,2048]{1,0:T(8,128)(2,1)}, f32[8,2048]{1,0:T(8,128)S(1)}) custom-call(s32[8]{0:T(128)S(1)} %stack.87.at_ref, bf16[768,2048]{1,0:T(8,128)(2,1)S(1)} %copy-done, bf16[2048,256]{1,0:T(8,128)(2,1)S(1)} %copy-done.10, ...), custom_call_target="tpu_custom_call", output_to_operand_aliasing={{0}: (16, {}), {1}: (17, {}), {2}: (18, {})} | custom-call | flops 1966080000 | bytes 3145728 | tf_op jit(solution)/shard_map/gate/pallas_call | solution.py:285
  150.2 5.4 %outer.2 = (f32[2,512,256]{2,1,0:T(8,128)S(1)}, f32[2,512,256]{2,1,0:T(8,128)S(1)}, f32[2,512,256]{2,1,0:T(8,128)S(1)}, f32[1,512,256]{2,1,0:T(8,128)S(1)}, f32[1,512,256]{2,1,0:T(8,128)S(1)}) custom-call(s32[4]{0:T(128)S(1)} %pad_add_fusion.1.at_ref, bf16[1024,768]{1,0:T(8,128)(2,1)} %collective-permute-done.14.hidden_ref, f32[8,1024,256]{2,1,0:T(8,128)S(1)} %bitcast.58, ...), custom_call_target="tpu_custom_call" | custom-call | flops 1610612736 | bytes 3145728 | tf_op jit(solution)/shard_map/outer/pallas_call | solution.py:179
  155.8 2.7 %collective-permute-start.20 = (bf16[512,256]{1,0:T(8,128)(2,1)S(1)}, bf16[512,256]{1,0:T(8,128)(2,1)S(1)}, u32[]{:S(2)}, u32[]{:S(2)}) collective-permute-start(bf16[512,256]{1,0:T(8,128)(2,1)S(1)} %get-tuple-element.63), channel_id=1, source_target_pairs={{0,4},{2,6},{4,8},{6,10},{8,12},{10,14},{12,0},{14,2},{1,5},{3,7},... | collective-permute-start | bytes 786440 | tf_op jit(solution)/shard_map/ppermute | solution.py:26
  158.5 2.4 %collective-permute-start.19 = (bf16[512,256]{1,0:T(8,128)(2,1)S(1)}, bf16[512,256]{1,0:T(8,128)(2,1)S(1)}, u32[]{:S(2)}, u32[]{:S(2)}) collective-permute-start(bf16[512,256]{1,0:T(8,128)(2,1)S(1)} %get-tuple-element.62), channel_id=1, source_target_pairs={{0,12},{2,14},{4,0},{6,2},{8,4},{10,6},{12,8},{14,10},{1,13},{3,15... | collective-permute-start | bytes 786440 | tf_op jit(solution)/shard_map/ppermute | solution.py:26
  160.9 8.2 %collective-permute-done.23 = bf16[2,512,256]{2,1,0:T(8,128)(2,1)S(1)} collective-permute-done((bf16[2,512,256]{2,1,0:T(8,128)(2,1)S(1)}, bf16[2,512,256]{2,1,0:T(8,128)(2,1)S(1)}, u32[]{:S(2)}, u32[]{:S(2)}) %collective-permute-start.23) | collective-permute-done | bytes 524320 | tf_op jit(solution)/shard_map/ppermute | solution.py:20
  169.3 3.1 %collective-permute-start.26 = (bf16[512,256]{1,0:T(8,128)(2,1)S(1)}, bf16[512,256]{1,0:T(8,128)(2,1)S(1)}, u32[]{:S(2)}, u32[]{:S(2)}) collective-permute-start(bf16[512,256]{1,0:T(8,128)(2,1)S(1)} %get-tuple-element.65), channel_id=1, source_target_pairs={{0,4},{2,6},{4,8},{6,10},{8,12},{10,14},{12,0},{14,2},{1,5},{3,7},... | collective-permute-start | bytes 786440 | tf_op jit(solution)/shard_map/ppermute | solution.py:26
  173.9 8.8 %gate.7 = (bf16[768,2048]{1,0:T(8,128)(2,1)}, bf16[768,2048]{1,0:T(8,128)(2,1)}, f32[8,2048]{1,0:T(8,128)S(1)}) custom-call(s32[8]{0:T(128)S(1)} %stack.87.at_ref, bf16[768,2048]{1,0:T(8,128)(2,1)S(1)} %copy-done, bf16[2048,256]{1,0:T(8,128)(2,1)S(1)} %copy-done.10, ...), custom_call_target="tpu_custom_call", output_to_operand_aliasing={{0}: (16, {}), {1}: (17, {}), {2}: (18, {})} | custom-call | flops 1966080000 | bytes 3145728 | tf_op jit(solution)/shard_map/gate/pallas_call | solution.py:285
  184.1 2.7 %collective-permute-start.24 = (bf16[512,256]{1,0:T(8,128)(2,1)S(1)}, bf16[512,256]{1,0:T(8,128)(2,1)S(1)}, u32[]{:S(2)}, u32[]{:S(2)}) collective-permute-start(bf16[512,256]{1,0:T(8,128)(2,1)S(1)} %get-tuple-element.64), channel_id=1, source_target_pairs={{0,12},{2,14},{4,0},{6,2},{8,4},{10,6},{12,8},{14,10},{1,13},{3,15... | collective-permute-start | bytes 786440 | tf_op jit(solution)/shard_map/ppermute | solution.py:26
  187.2 2.0 collective-permute-done.22
  189.1 3.8 %collective-permute-done.24 = bf16[512,256]{1,0:T(8,128)(2,1)S(1)} collective-permute-done((bf16[512,256]{1,0:T(8,128)(2,1)S(1)}, bf16[512,256]{1,0:T(8,128)(2,1)S(1)}, u32[]{:S(2)}, u32[]{:S(2)}) %collective-permute-start.24) | collective-permute-done | bytes 262176 | tf_op jit(solution)/shard_map/ppermute | solution.py:26
  193.0 3.3 %collective-permute-done.27 = bf16[512,256]{1,0:T(8,128)(2,1)S(1)} collective-permute-done((bf16[512,256]{1,0:T(8,128)(2,1)S(1)}, bf16[512,256]{1,0:T(8,128)(2,1)S(1)}, u32[]{:S(2)}, u32[]{:S(2)}) %collective-permute-start.27) | collective-permute-done | bytes 262176 | tf_op jit(solution)/shard_map/ppermute | solution.py:26
  196.5 3.0 %collective-permute-start.28 = (f32[8,2176]{1,0:T(8,128)S(1)}, f32[8,2176]{1,0:T(8,128)S(1)}, u32[]{:S(2)}, u32[]{:S(2)}) collective-permute-start(f32[8,2176]{1,0:T(8,128)S(1)} %maximum_maximum_fusion), channel_id=1, source_target_pairs={{0,8},{2,10},{4,12},{6,14},{8,0},{10,2},{12,4},{14,6},{16,24},{18,... | collective-permute-start | bytes 208904 | tf_op jit(solution)/shard_map/ppermute | solution.py:20
  199.6 1.5 collective-permute-start.30
  201.9 2.0 collective-permute-done.29
  203.9 1.9 collective-permute-done.30
  209.4 1.5 collective-permute-start.34
  211.4 2.4 %collective-permute-done.33 = f32[8,2176]{1,0:T(8,128)S(1)} collective-permute-done((f32[8,2176]{1,0:T(8,128)S(1)}, f32[8,2176]{1,0:T(8,128)S(1)}, u32[]{:S(2)}, u32[]{:S(2)}) %collective-permute-start.33) | collective-permute-done | bytes 69664 | tf_op jit(solution)/shard_map/ppermute | solution.py:20
  215.8 3.2 %collective-permute-done.34 = f32[512,256]{1,0:T(8,128)S(1)} collective-permute-done((f32[512,256]{1,0:T(8,128)S(1)}, f32[512,256]{1,0:T(8,128)S(1)}, u32[]{:S(2)}, u32[]{:S(2)}) %collective-permute-start.34) | collective-permute-done | bytes 524320 | tf_op jit(solution)/shard_map/ppermute | solution.py:20
  219.1 5.5 %collective-permute-done.35 = f32[512,256]{1,0:T(8,128)S(1)} collective-permute-done((f32[512,256]{1,0:T(8,128)S(1)}, f32[512,256]{1,0:T(8,128)S(1)}, u32[]{:S(2)}, u32[]{:S(2)}) %collective-permute-start.35) | collective-permute-done | bytes 524320 | tf_op jit(solution)/shard_map/ppermute | solution.py:20
  (98 shorter events, 20.1 us)
Async XLA Ops:
  0.6 13.2 %copy-start.3 = (bf16[768,2048]{1,0:T(8,128)(2,1)S(1)}, bf16[768,2048]{1,0:T(8,128)(2,1)}, u32[]{:S(2)}) copy-start(bf16[768,2048]{1,0:T(8,128)(2,1)} %gate_ref.3) | copy-start | bytes 9437188
  0.7 13.2 %copy-start.11 = (f32[3,2048]{1,0:T(4,128)S(1)}, f32[3,2048]{1,0:T(4,128)}, u32[]{:S(2)}) copy-start(f32[3,2048]{1,0:T(4,128)} %tg_ref.3) | copy-start | bytes 73732
  0.7 13.2 %copy-start.12 = (f32[3,2048]{1,0:T(4,128)S(1)}, f32[3,2048]{1,0:T(4,128)}, u32[]{:S(2)}) copy-start(f32[3,2048]{1,0:T(4,128)} %tl_ref.3) | copy-start | bytes 73732
  0.7 13.2 %copy-start.13 = (f32[2048]{0:T(1024)S(1)}, f32[2048]{0:T(1024)}, u32[]{:S(2)}) copy-start(f32[2048]{0:T(1024)} %param.12) | copy-start | bytes 24580
  0.7 13.2 %copy-start.14 = (f32[2048]{0:T(1024)S(1)}, f32[2048]{0:T(1024)}, u32[]{:S(2)}) copy-start(f32[2048]{0:T(1024)} %param.13) | copy-start | bytes 24580
  3.6 38.5 %collective-permute-start.15 = (bf16[384,2048]{1,0:T(8,128)(2,1)}, bf16[384,2048]{1,0:T(8,128)(2,1)}, u32[]{:S(2)}, u32[]{:S(2)}) collective-permute-start(bf16[384,2048]{1,0:T(8,128)(2,1)} %constant_dynamic-slice_fusion), channel_id=1, source_target_pairs={{0,16},{16,0},{1,17},{17,1},{2,18},{18,2},{3,19},{19,3},{4,20},{20... | collective-permute-start | bytes 4718600 | tf_op jit(solution)/shard_map/ppermute | solution.py:20
  8.4 34.5 %collective-permute-start.7 = (bf16[1024,256]{1,0:T(8,128)(2,1)}, bf16[1024,256]{1,0:T(8,128)(2,1)}, u32[]{:S(2)}, u32[]{:S(2)}) collective-permute-start(bf16[1024,256]{1,0:T(8,128)(2,1)} %slice.53), channel_id=1, source_target_pairs={{0,4},{2,6},{4,8},{6,10},{8,12},{10,14},{12,0},{14,2},{1,5},{3,7},... | collective-permute-start | bytes 1572872 | tf_op jit(solution)/shard_map/ppermute | solution.py:26
  10.0 35.1 %collective-permute-start.8 = (bf16[1024,256]{1,0:T(8,128)(2,1)}, bf16[1024,256]{1,0:T(8,128)(2,1)}, u32[]{:S(2)}, u32[]{:S(2)}) collective-permute-start(bf16[1024,256]{1,0:T(8,128)(2,1)} %slice.53), channel_id=1, source_target_pairs={{0,12},{2,14},{4,0},{6,2},{8,4},{10,6},{12,8},{14,10},{1,13},{3,15... | collective-permute-start | bytes 1572872 | tf_op jit(solution)/shard_map/ppermute | solution.py:26
  12.2 34.9 %collective-permute-start.10 = (bf16[1024,256]{1,0:T(8,128)(2,1)}, bf16[1024,256]{1,0:T(8,128)(2,1)}, u32[]{:S(2)}, u32[]{:S(2)}) collective-permute-start(bf16[1024,256]{1,0:T(8,128)(2,1)} %slice.53), channel_id=1, source_target_pairs={{0,2},{2,0},{4,6},{6,4},{8,10},{10,8},{12,14},{14,12},{1,3},{3,1},... | collective-permute-start | bytes 1572872 | tf_op jit(solution)/shard_map/ppermute | solution.py:20
  15.7 26.4 %copy-start.9 = (bf16[2048,256]{1,0:T(8,128)(2,1)S(1)}, bf16[2048,256]{1,0:T(8,128)(2,1)}, u32[]{:S(2)}) copy-start(bf16[2048,256]{1,0:T(8,128)(2,1)} %refs_0_.7) | copy-start | bytes 3145732
  21.7 85.1 %collective-permute-start.14 = (bf16[1024,768]{1,0:T(8,128)(2,1)}, bf16[1024,768]{1,0:T(8,128)(2,1)}, u32[]{:S(2)}, u32[]{:S(2)}) collective-permute-start(bf16[1024,768]{1,0:T(8,128)(2,1)} %hidden.2), channel_id=1, source_target_pairs={{0,16},{16,0},{1,17},{17,1},{2,18},{18,2},{3,19},{19,3},{4,20},{20... | collective-permute-start | bytes 4718600 | tf_op jit(solution)/shard_map/ppermute | solution.py:20
  42.1 66.0 %collective-permute-start.16 = (bf16[384,2048]{1,0:T(8,128)(2,1)}, bf16[384,2048]{1,0:T(8,128)(2,1)}, u32[]{:S(2)}, u32[]{:S(2)}) collective-permute-start(bf16[384,2048]{1,0:T(8,128)(2,1)} %collective-permute-done.15.refs_0_), channel_id=1, source_target_pairs={{0,1},{1,0},{2,3},{3,2},{4,5},{5,4},{6,7},{7,6},{8,9},{9,8},{10,11... | collective-permute-start | bytes 4718600 | tf_op jit(solution)/shard_map/ppermute | solution.py:20
  42.9 17.3 %collective-permute-start = (bf16[1024,256]{1,0:T(8,128)(2,1)}, bf16[1024,256]{1,0:T(8,128)(2,1)}, u32[]{:S(2)}, u32[]{:S(2)}) collective-permute-start(bf16[1024,256]{1,0:T(8,128)(2,1)} %slice.52), channel_id=1, source_target_pairs={{0,4},{2,6},{4,8},{6,10},{8,12},{10,14},{12,0},{14,2},{1,5},{3,7},... | collective-permute-start | bytes 1572872 | tf_op jit(solution)/shard_map/ppermute | solution.py:26
  45.1 25.6 %collective-permute-start.1 = (bf16[1024,256]{1,0:T(8,128)(2,1)}, bf16[1024,256]{1,0:T(8,128)(2,1)}, u32[]{:S(2)}, u32[]{:S(2)}) collective-permute-start(bf16[1024,256]{1,0:T(8,128)(2,1)} %slice.52), channel_id=1, source_target_pairs={{0,12},{2,14},{4,0},{6,2},{8,4},{10,6},{12,8},{14,10},{1,13},{3,15... | collective-permute-start | bytes 1572872 | tf_op jit(solution)/shard_map/ppermute | solution.py:26
  47.1 35.4 %collective-permute-start.9 = (bf16[1024,256]{1,0:T(8,128)(2,1)}, bf16[1024,256]{1,0:T(8,128)(2,1)}, u32[]{:S(2)}, u32[]{:S(2)}) collective-permute-start(bf16[1024,256]{1,0:T(8,128)(2,1)} %collective-permute-done.7.refs_1_), channel_id=1, source_target_pairs={{0,4},{2,6},{4,8},{6,10},{8,12},{10,14},{12,0},{14,2},{1,5},{3,7},... | collective-permute-start | bytes 1572872 | tf_op jit(solution)/shard_map/ppermute | solution.py:26
  60.2 32.9 %collective-permute-start.11 = (bf16[1024,256]{1,0:T(8,128)(2,1)}, bf16[1024,256]{1,0:T(8,128)(2,1)}, u32[]{:S(2)}, u32[]{:S(2)}) collective-permute-start(bf16[1024,256]{1,0:T(8,128)(2,1)} %collective-permute-done.7.refs_1_), channel_id=1, source_target_pairs={{0,2},{2,0},{4,6},{6,4},{8,10},{10,8},{12,14},{14,12},{1,3},{3,1},... | collective-permute-start | bytes 1572872 | tf_op jit(solution)/shard_map/ppermute | solution.py:20
  70.7 32.1 %collective-permute-start.12 = (bf16[1024,256]{1,0:T(8,128)(2,1)}, bf16[1024,256]{1,0:T(8,128)(2,1)}, u32[]{:S(2)}, u32[]{:S(2)}) collective-permute-start(bf16[1024,256]{1,0:T(8,128)(2,1)} %collective-permute-done.8.refs_2_), channel_id=1, source_target_pairs={{0,2},{2,0},{4,6},{6,4},{8,10},{10,8},{12,14},{14,12},{1,3},{3,1},... | collective-permute-start | bytes 1572872 | tf_op jit(solution)/shard_map/ppermute | solution.py:20
  82.5 21.8 %collective-permute-start.4 = (bf16[1024,256]{1,0:T(8,128)(2,1)}, bf16[1024,256]{1,0:T(8,128)(2,1)}, u32[]{:S(2)}, u32[]{:S(2)}) collective-permute-start(bf16[1024,256]{1,0:T(8,128)(2,1)} %collective-permute-done.refs_1_), channel_id=1, source_target_pairs={{0,2},{2,0},{4,6},{6,4},{8,10},{10,8},{12,14},{14,12},{1,3},{3,1},... | collective-permute-start | bytes 1572872 | tf_op jit(solution)/shard_map/ppermute | solution.py:20
  88.0 5.7 %copy-start = (bf16[768,2048]{1,0:T(8,128)(2,1)S(1)}, bf16[768,2048]{1,0:T(8,128)(2,1)}, u32[]{:S(2)}) copy-start(bf16[768,2048]{1,0:T(8,128)(2,1)} %tokens_ref.9) | copy-start | bytes 9437188
  93.1 26.2 %collective-permute-start.13 = (bf16[1024,256]{1,0:T(8,128)(2,1)}, bf16[1024,256]{1,0:T(8,128)(2,1)}, u32[]{:S(2)}, u32[]{:S(2)}) collective-permute-start(bf16[1024,256]{1,0:T(8,128)(2,1)} %collective-permute-done.9.refs_3_), channel_id=1, source_target_pairs={{0,2},{2,0},{4,6},{6,4},{8,10},{10,8},{12,14},{14,12},{1,3},{3,1},... | collective-permute-start | bytes 1572872 | tf_op jit(solution)/shard_map/ppermute | solution.py:20
  102.7 35.2 %collective-permute-start.3 = (bf16[1024,256]{1,0:T(8,128)(2,1)}, bf16[1024,256]{1,0:T(8,128)(2,1)}, u32[]{:S(2)}, u32[]{:S(2)}) collective-permute-start(bf16[1024,256]{1,0:T(8,128)(2,1)} %slice.52), channel_id=1, source_target_pairs={{0,2},{2,0},{4,6},{6,4},{8,10},{10,8},{12,14},{14,12},{1,3},{3,1},... | collective-permute-start | bytes 1572872 | tf_op jit(solution)/shard_map/ppermute | solution.py:20
  104.3 33.7 %collective-permute-start.2 = (bf16[1024,256]{1,0:T(8,128)(2,1)}, bf16[1024,256]{1,0:T(8,128)(2,1)}, u32[]{:S(2)}, u32[]{:S(2)}) collective-permute-start(bf16[1024,256]{1,0:T(8,128)(2,1)} %collective-permute-done.refs_1_), channel_id=1, source_target_pairs={{0,4},{2,6},{4,8},{6,10},{8,12},{10,14},{12,0},{14,2},{1,5},{3,7},... | collective-permute-start | bytes 1572872 | tf_op jit(solution)/shard_map/ppermute | solution.py:26
  106.8 31.2 %collective-permute-start.5 = (bf16[1024,256]{1,0:T(8,128)(2,1)}, bf16[1024,256]{1,0:T(8,128)(2,1)}, u32[]{:S(2)}, u32[]{:S(2)}) collective-permute-start(bf16[1024,256]{1,0:T(8,128)(2,1)} %collective-permute-done.1.refs_2_), channel_id=1, source_target_pairs={{0,2},{2,0},{4,6},{6,4},{8,10},{10,8},{12,14},{14,12},{1,3},{3,1},... | collective-permute-start | bytes 1572872 | tf_op jit(solution)/shard_map/ppermute | solution.py:20
  108.1 29.9 %collective-permute-start.6 = (bf16[1024,256]{1,0:T(8,128)(2,1)}, bf16[1024,256]{1,0:T(8,128)(2,1)}, u32[]{:S(2)}, u32[]{:S(2)}) collective-permute-start(bf16[1024,256]{1,0:T(8,128)(2,1)} %collective-permute-done.4.refs_5_), channel_id=1, source_target_pairs={{0,4},{2,6},{4,8},{6,10},{8,12},{10,14},{12,0},{14,2},{1,5},{3,7},... | collective-permute-start | bytes 1572872 | tf_op jit(solution)/shard_map/ppermute | solution.py:26
  113.7 6.6 %copy-start.5 = (bf16[768,2048]{1,0:T(8,128)(2,1)S(1)}, bf16[768,2048]{1,0:T(8,128)(2,1)}, u32[]{:S(2)}) copy-start(bf16[768,2048]{1,0:T(8,128)(2,1)} %gate_ref.3) | copy-start | bytes 9437188
  113.7 6.6 %copy-start.8 = (bf16[768,2048]{1,0:T(8,128)(2,1)S(1)}, bf16[768,2048]{1,0:T(8,128)(2,1)}, u32[]{:S(2)}) copy-start(bf16[768,2048]{1,0:T(8,128)(2,1)} %linear_ref.3) | copy-start | bytes 9437188
  113.7 6.6 %copy-start.10 = (bf16[2048,256]{1,0:T(8,128)(2,1)S(1)}, bf16[2048,256]{1,0:T(8,128)(2,1)}, u32[]{:S(2)}) copy-start(bf16[2048,256]{1,0:T(8,128)(2,1)} %refs_0_.7) | copy-start | bytes 3145732
  119.3 36.3 %collective-permute-start.18 = (bf16[2,512,256]{2,1,0:T(8,128)(2,1)S(1)}, bf16[2,512,256]{2,1,0:T(8,128)(2,1)S(1)}, u32[]{:S(2)}, u32[]{:S(2)}) collective-permute-start(bf16[2,512,256]{2,1,0:T(8,128)(2,1)S(1)} %get-tuple-element.47), channel_id=1, source_target_pairs={{0,2},{2,0},{4,6},{6,4},{8,10},{10,8},{12,14},{14,12},{1,3},{3,1},... | collective-permute-start | bytes 1572872 | tf_op jit(solution)/shard_map/ppermute | solution.py:20
  138.0 12.2 %slice-start = ((s8[8388608]{0:T(1024)(128)(4,1)}), s8[4194304]{0:T(1024)(128)(4,1)S(1)}, s32[]{:S(2)}) async-start(s8[8388608]{0:T(1024)(128)(4,1)} %bitcast.57), calls=%async_computation | async-start | bytes 8388608
  138.0 12.2 %slice-start.1 = ((s8[8388608]{0:T(1024)(128)(4,1)}), s8[4194304]{0:T(1024)(128)(4,1)S(1)}, s32[]{:S(2)}) async-start(s8[8388608]{0:T(1024)(128)(4,1)} %bitcast.57), calls=%async_computation.1 | async-start | bytes 8388608
  147.1 25.3 %collective-permute-start.17 = (bf16[2,512,256]{2,1,0:T(8,128)(2,1)S(1)}, bf16[2,512,256]{2,1,0:T(8,128)(2,1)S(1)}, u32[]{:S(2)}, u32[]{:S(2)}) collective-permute-start(bf16[2,512,256]{2,1,0:T(8,128)(2,1)S(1)} %get-tuple-element.45), channel_id=1, source_target_pairs={{0,2},{2,0},{4,6},{6,4},{8,10},{10,8},{12,14},{14,12},{1,3},{3,1},... | collective-permute-start | bytes 1572872 | tf_op jit(solution)/shard_map/ppermute | solution.py:20
  148.2 20.9 %collective-permute-start.23 = (bf16[2,512,256]{2,1,0:T(8,128)(2,1)S(1)}, bf16[2,512,256]{2,1,0:T(8,128)(2,1)S(1)}, u32[]{:S(2)}, u32[]{:S(2)}) collective-permute-start(bf16[2,512,256]{2,1,0:T(8,128)(2,1)S(1)} %get-tuple-element.51), channel_id=1, source_target_pairs={{0,2},{2,0},{4,6},{6,4},{8,10},{10,8},{12,14},{14,12},{1,3},{3,1},... | collective-permute-start | bytes 1572872 | tf_op jit(solution)/shard_map/ppermute | solution.py:20
  149.1 34.9 %collective-permute-start.25 = (bf16[1,512,256]{2,1,0:T(8,128)(2,1)S(1)}, bf16[1,512,256]{2,1,0:T(8,128)(2,1)S(1)}, u32[]{:S(2)}, u32[]{:S(2)}) collective-permute-start(bf16[1,512,256]{2,1,0:T(8,128)(2,1)S(1)} %get-tuple-element.53), channel_id=1, source_target_pairs={{0,2},{2,0},{4,6},{6,4},{8,10},{10,8},{12,14},{14,12},{1,3},{3,1},... | collective-permute-start | bytes 786440 | tf_op jit(solution)/shard_map/ppermute | solution.py:20
  155.8 16.7 %collective-permute-start.20 = (bf16[512,256]{1,0:T(8,128)(2,1)S(1)}, bf16[512,256]{1,0:T(8,128)(2,1)S(1)}, u32[]{:S(2)}, u32[]{:S(2)}) collective-permute-start(bf16[512,256]{1,0:T(8,128)(2,1)S(1)} %get-tuple-element.63), channel_id=1, source_target_pairs={{0,4},{2,6},{4,8},{6,10},{8,12},{10,14},{12,0},{14,2},{1,5},{3,7},... | collective-permute-start | bytes 786440 | tf_op jit(solution)/shard_map/ppermute | solution.py:26
  158.5 28.4 %collective-permute-start.19 = (bf16[512,256]{1,0:T(8,128)(2,1)S(1)}, bf16[512,256]{1,0:T(8,128)(2,1)S(1)}, u32[]{:S(2)}, u32[]{:S(2)}) collective-permute-start(bf16[512,256]{1,0:T(8,128)(2,1)S(1)} %get-tuple-element.62), channel_id=1, source_target_pairs={{0,12},{2,14},{4,0},{6,2},{8,4},{10,6},{12,8},{14,10},{1,13},{3,15... | collective-permute-start | bytes 786440 | tf_op jit(solution)/shard_map/ppermute | solution.py:26
  169.3 17.5 %collective-permute-start.26 = (bf16[512,256]{1,0:T(8,128)(2,1)S(1)}, bf16[512,256]{1,0:T(8,128)(2,1)S(1)}, u32[]{:S(2)}, u32[]{:S(2)}) collective-permute-start(bf16[512,256]{1,0:T(8,128)(2,1)S(1)} %get-tuple-element.65), channel_id=1, source_target_pairs={{0,4},{2,6},{4,8},{6,10},{8,12},{10,14},{12,0},{14,2},{1,5},{3,7},... | collective-permute-start | bytes 786440 | tf_op jit(solution)/shard_map/ppermute | solution.py:26
  172.6 14.4 %collective-permute-start.21 = (bf16[512,256]{1,0:T(8,128)(2,1)S(1)}, bf16[512,256]{1,0:T(8,128)(2,1)S(1)}, u32[]{:S(2)}, u32[]{:S(2)}) collective-permute-start(bf16[512,256]{1,0:T(8,128)(2,1)S(1)} %fusion.1), channel_id=1, source_target_pairs={{0,4},{2,6},{4,8},{6,10},{8,12},{10,14},{12,0},{14,2},{1,5},{3,7},... | collective-permute-start | bytes 786440 | tf_op jit(solution)/shard_map/ppermute | solution.py:26
  182.7 6.4 %collective-permute-start.22 = (bf16[1,512,256]{2,1,0:T(8,128)(2,1)S(1)}, bf16[1,512,256]{2,1,0:T(8,128)(2,1)S(1)}, u32[]{:S(2)}, u32[]{:S(2)}) collective-permute-start(bf16[1,512,256]{2,1,0:T(8,128)(2,1)S(1)} %get-tuple-element.49), channel_id=1, source_target_pairs={{0,2},{2,0},{4,6},{6,4},{8,10},{10,8},{12,14},{14,12},{1,3},{3,1},... | collective-permute-start | bytes 786440 | tf_op jit(solution)/shard_map/ppermute | solution.py:20
  184.1 8.9 %collective-permute-start.24 = (bf16[512,256]{1,0:T(8,128)(2,1)S(1)}, bf16[512,256]{1,0:T(8,128)(2,1)S(1)}, u32[]{:S(2)}, u32[]{:S(2)}) collective-permute-start(bf16[512,256]{1,0:T(8,128)(2,1)S(1)} %get-tuple-element.64), channel_id=1, source_target_pairs={{0,12},{2,14},{4,0},{6,2},{8,4},{10,6},{12,8},{14,10},{1,13},{3,15... | collective-permute-start | bytes 786440 | tf_op jit(solution)/shard_map/ppermute | solution.py:26
  186.9 9.4 %collective-permute-start.27 = (bf16[512,256]{1,0:T(8,128)(2,1)S(1)}, bf16[512,256]{1,0:T(8,128)(2,1)S(1)}, u32[]{:S(2)}, u32[]{:S(2)}) collective-permute-start(bf16[512,256]{1,0:T(8,128)(2,1)S(1)} %fusion.4), channel_id=1, source_target_pairs={{0,4},{2,6},{4,8},{6,10},{8,12},{10,14},{12,0},{14,2},{1,5},{3,7},... | collective-permute-start | bytes 786440 | tf_op jit(solution)/shard_map/ppermute | solution.py:26
  196.5 5.3 %collective-permute-start.28 = (f32[8,2176]{1,0:T(8,128)S(1)}, f32[8,2176]{1,0:T(8,128)S(1)}, u32[]{:S(2)}, u32[]{:S(2)}) collective-permute-start(f32[8,2176]{1,0:T(8,128)S(1)} %maximum_maximum_fusion), channel_id=1, source_target_pairs={{0,8},{2,10},{4,12},{6,14},{8,0},{10,2},{12,4},{14,6},{16,24},{18,... | collective-permute-start | bytes 208904 | tf_op jit(solution)/shard_map/ppermute | solution.py:20
  199.6 4.3 %collective-permute-start.29 = (f32[8,2176]{1,0:T(8,128)S(1)}, f32[8,2176]{1,0:T(8,128)S(1)}, u32[]{:S(2)}, u32[]{:S(2)}) collective-permute-start(f32[8,2176]{1,0:T(8,128)S(1)} %maximum_maximum_fusion), channel_id=1, source_target_pairs={{0,4},{2,6},{4,0},{6,2},{8,12},{10,14},{12,8},{14,10},{16,20},{18,... | collective-permute-start | bytes 208904 | tf_op jit(solution)/shard_map/ppermute | solution.py:20
  199.6 6.2 %collective-permute-start.30 = (f32[8,2176]{1,0:T(8,128)S(1)}, f32[8,2176]{1,0:T(8,128)S(1)}, u32[]{:S(2)}, u32[]{:S(2)}) collective-permute-start(f32[8,2176]{1,0:T(8,128)S(1)} %maximum_maximum_fusion), channel_id=1, source_target_pairs={{0,12},{2,14},{4,8},{6,10},{8,4},{10,6},{12,0},{14,2},{16,28},{18,... | collective-permute-start | bytes 208904 | tf_op jit(solution)/shard_map/ppermute | solution.py:20
  205.8 5.6 %collective-permute-start.31 = (f32[8,2176]{1,0:T(8,128)S(1)}, f32[8,2176]{1,0:T(8,128)S(1)}, u32[]{:S(2)}, u32[]{:S(2)}) collective-permute-start(f32[8,2176]{1,0:T(8,128)S(1)} %add_add_fusion), channel_id=1, source_target_pairs={{0,2},{2,0},{4,6},{6,4},{8,10},{10,8},{12,14},{14,12},{16,18},{18,... | collective-permute-start | bytes 208904 | tf_op jit(solution)/shard_map/ppermute | solution.py:20
  206.4 5.1 %collective-permute-start.32 = (f32[8,2176]{1,0:T(8,128)S(1)}, f32[8,2176]{1,0:T(8,128)S(1)}, u32[]{:S(2)}, u32[]{:S(2)}) collective-permute-start(f32[8,2176]{1,0:T(8,128)S(1)} %add_add_fusion), channel_id=1, source_target_pairs={{0,16},{2,18},{4,20},{6,22},{8,24},{10,26},{12,28},{14,30},{16,0},... | collective-permute-start | bytes 208904 | tf_op jit(solution)/shard_map/ppermute | solution.py:20
  207.9 6.0 %collective-permute-start.33 = (f32[8,2176]{1,0:T(8,128)S(1)}, f32[8,2176]{1,0:T(8,128)S(1)}, u32[]{:S(2)}, u32[]{:S(2)}) collective-permute-start(f32[8,2176]{1,0:T(8,128)S(1)} %add_add_fusion), channel_id=1, source_target_pairs={{0,18},{2,16},{4,22},{6,20},{8,26},{10,24},{12,30},{14,28},{16,2},... | collective-permute-start | bytes 208904 | tf_op jit(solution)/shard_map/ppermute | solution.py:20
  209.4 9.6 %collective-permute-start.34 = (f32[512,256]{1,0:T(8,128)S(1)}, f32[512,256]{1,0:T(8,128)S(1)}, u32[]{:S(2)}, u32[]{:S(2)}) collective-permute-start(f32[512,256]{1,0:T(8,128)S(1)} %get-tuple-element.55), channel_id=1, source_target_pairs={{0,16},{16,0},{1,17},{17,1},{2,18},{18,2},{3,19},{19,3},{4,20},{20... | collective-permute-start | bytes 1572872 | tf_op jit(solution)/shard_map/ppermute | solution.py:20
  210.9 13.8 %collective-permute-start.35 = (f32[512,256]{1,0:T(8,128)S(1)}, f32[512,256]{1,0:T(8,128)S(1)}, u32[]{:S(2)}, u32[]{:S(2)}) collective-permute-start(f32[512,256]{1,0:T(8,128)S(1)} %get-tuple-element.57), channel_id=1, source_target_pairs={{0,16},{16,0},{1,17},{17,1},{2,18},{18,2},{3,19},{19,3},{4,20},{20... | collective-permute-start | bytes 1572872 | tf_op jit(solution)/shard_map/ppermute | solution.py:20
  (5 other events, 12.4 us)
where the time goes:
time: 227 us; the launch traced here: 226 us
  waiting for transfers between devices  85.2 us (38%)
  Pallas kernels  63.2 us (28%)
  starting transfers between devices  53.7 us (24%)
  local copies, waits for them, and re-layouts  19.5 us (9%)
  other arithmetic  3.52 us (2%)
    ppermute x23, waiting for transfers between devices, swap(): return lax.ppermute(value, axis, [(i, i ^ distance) for i in range(size)])  46 us
    ppermute x13, waiting for transfers between devices, ring(): return lax.ppermute(value, 'fs', pairs)  39.2 us
    pallas_call x4, Pallas kernels, gate_part(): pl.pallas_call(functools.partial(gate_kernel, size, aliased), grid_spec=p...  35.6 us
    ppermute x23, starting transfers between devices, swap(): return lax.ppermute(value, axis, [(i, i ^ distance) for i in range(size)])  28.8 us
    ppermute x13, starting transfers between devices, ring(): return lax.ppermute(value, 'fs', pairs)  25 us
    unnamed x34, local copies, waits for them, and re-layouts  12.4 us
    pallas_call x2, Pallas kernels, hidden_half(): pl.pallas_call(functools.partial(hidden_kernel, block_rows), grid_spec=pl...  11 us
    pallas_call x2, Pallas kernels, outer_blocks(): pl.pallas_call(functools.partial(outer_kernel, groups, kind, len(shares))...  10.9 us
  transfers between devices with their start and end apart: 36, of which 14 were waited for; matrix products, arithmetic and copies ran while one was open for 3% of the time, Pallas kernels for 28%

commit v1 on v0

--- a/solution.py
+++ b/solution.py
@@ -77,7 +77,7 @@
             made[pl.ds(to, step), cols] = (g * jax.nn.sigmoid(g) * l).astype(BF16)
             return carry
 
-        lax.fori_loop(0, rows // step, body, 0, unroll=2)
+        lax.fori_loop(0, rows // step, body, 0, unroll=4)
     out_ref[...] = made[...].T
 
 
@@ -253,8 +253,9 @@
             linear_pre = tl_ref[0:1, here] * l2 + tl_ref[1:2, here] * l1 + tl_ref[2:3, here] * l0 + bl_ref[0:1, here]
             sigma = jax.nn.sigmoid(gate_pre)
             grad = grads[pl.ds(start, step), here]
-            d_gate = grad * linear_pre * sigma * (1.0 + gate_pre * (1.0 - sigma))
-            d_linear = grad * (gate_pre * sigma)
+            silu = gate_pre * sigma
+            d_gate = grad * linear_pre * (sigma + silu * (1.0 - sigma))
+            d_linear = grad * silu
             gate_out[pl.ds(start, step), here] = back(d_gate, later_g, tg_ref).astype(BF16)
             linear_out[pl.ds(start, step), here] = back(d_linear, later_l, tl_ref).astype(BF16)
             terms = (d_gate * g2, d_gate * g1, d_gate * g0, d_linear * l2, d_linear * l1, d_linear * l0, d_gate, d_linear)

time: 227 us -> 228 us (level)
  transfers between devices with their start and end apart: 36 -> 36, of which waited for: 14 -> 14; matrix products, arithmetic and copies ran while one was open for 3% -> 3% of each run, Pallas kernels for 28% -> 27%
where the time goes in v1:
time: 228 us; the launch traced here: 227 us
  waiting for transfers between devices  86.1 us (38%)
  Pallas kernels  61.9 us (27%)
  starting transfers between devices  55.4 us (24%)
  local copies, waits for them, and re-layouts  19.5 us (9%)
  other arithmetic  3.52 us (2%)
    ppermute x23, waiting for transfers between devices, swap(): return lax.ppermute(value, axis, [(i, i ^ distance) for i in range(size)])  47 us
    ppermute x13, waiting for transfers between devices, ring(): return lax.ppermute(value, 'fs', pairs)  39.1 us
    pallas_call x4, Pallas kernels, gate_part(): pl.pallas_call(functools.partial(gate_kernel, size, aliased), grid_spec=p...  34.6 us
    ppermute x23, starting transfers between devices, swap(): return lax.ppermute(value, axis, [(i, i ^ distance) for i in range(size)])  28.9 us
    ppermute x13, starting transfers between devices, ring(): return lax.ppermute(value, 'fs', pairs)  26.6 us
    unnamed x34, local copies, waits for them, and re-layouts  12.4 us
    pallas_call x2, Pallas kernels, outer_blocks(): pl.pallas_call(functools.partial(outer_kernel, groups, kind, len(shares))...  10.9 us
    pallas_call x2, Pallas kernels, hidden_half(): pl.pallas_call(functools.partial(hidden_kernel, block_rows), grid_spec=pl...  10.6 us
  transfers between devices with their start and end apart: 36, of which 14 were waited for; matrix products, arithmetic and copies ran while one was open for 3% of the time, Pallas kernels for 27%

profile of v1, /device:TPU:0, one launch (start us, length us, event | category | flops | bytes accessed | tf_op | source)
XLA Modules:
  0.0 227.4 jit_solution(13266566711054265496)
XLA Ops:
  0.7 2.9 %constant_dynamic-slice_fusion = bf16[384,2048]{1,0:T(8,128)(2,1)} fusion(bf16[768,2048]{1,0:T(8,128)(2,1)} %tokens_ref.9, s32[]{:T(128)S(6)} %select_n.107), kind=kLoop, calls=%fused_computation.34 | loop fusion | bytes 3145732 | tf_op jit(solution)/shard_map/dynamic_slice | solution.py:349
  3.6 3.0 %collective-permute-start.15 = (bf16[384,2048]{1,0:T(8,128)(2,1)}, bf16[384,2048]{1,0:T(8,128)(2,1)}, u32[]{:S(2)}, u32[]{:S(2)}) collective-permute-start(bf16[384,2048]{1,0:T(8,128)(2,1)} %constant_dynamic-slice_fusion), channel_id=1, source_target_pairs={{0,16},{16,0},{1,17},{17,1},{2,18},{18,2},{3,19},{19,3},{4,20},{20... | collective-permute-start | bytes 4718600 | tf_op jit(solution)/shard_map/ppermute | solution.py:20
  6.5 1.9 slice.53
  8.4 1.6 collective-permute-start.7
  10.0 2.2 collective-permute-start.8
  12.2 1.5 collective-permute-start.10
  13.9 1.9 copy-done.6
  15.7 5.7 %hidden.2 = bf16[1024,768]{1,0:T(8,128)(2,1)} custom-call(s32[2]{0:T(128)S(1)} %pad_add_fusion.at_ref, bf16[768,2048]{1,0:T(8,128)(2,1)S(1)} %copy-done.3, bf16[768,2048]{1,0:T(8,128)(2,1)S(1)} %copy-done.6, f32[3,2048]{1,0:T(4,128)S(1)} %copy-done.11, f32[3,2048]{1,0:T(4,128)S(1)} %copy-done.12, f32[1,2048]{1,0:T(1,128)S(1)} %bitcast.59, f32[1,2048]{1,0:T(1,128)S(1)} %bitcast.65), custom_call_target="tpu_custom_call" | custom-call | flops 2359296000 | bytes 4718592 | tf_op jit(solution)/shard_map/hidden/pallas_call | solution.py:92
  22.0 20.1 %collective-permute-done.15.refs_0_ = bf16[384,2048]{1,0:T(8,128)(2,1)} collective-permute-done((bf16[384,2048]{1,0:T(8,128)(2,1)}, bf16[384,2048]{1,0:T(8,128)(2,1)}, u32[]{:S(2)}, u32[]{:S(2)}) %collective-permute-start.15) | collective-permute-done | bytes 1572896 | tf_op jit(solution)/shard_map/ppermute | solution.py:20
  42.9 2.1 collective-permute-start
  45.1 2.1 collective-permute-start.1
  47.1 13.1 %collective-permute-done.refs_1_ = bf16[1024,256]{1,0:T(8,128)(2,1)} collective-permute-done((bf16[1024,256]{1,0:T(8,128)(2,1)}, bf16[1024,256]{1,0:T(8,128)(2,1)}, u32[]{:S(2)}, u32[]{:S(2)}) %collective-permute-start) | collective-permute-done | bytes 524320 | tf_op jit(solution)/shard_map/ppermute | solution.py:26
  60.2 1.7 collective-permute-start.11
  62.0 8.6 %collective-permute-done.1.refs_2_ = bf16[1024,256]{1,0:T(8,128)(2,1)} collective-permute-done((bf16[1024,256]{1,0:T(8,128)(2,1)}, bf16[1024,256]{1,0:T(8,128)(2,1)}, u32[]{:S(2)}, u32[]{:S(2)}) %collective-permute-start.1) | collective-permute-done | bytes 524320 | tf_op jit(solution)/shard_map/ppermute | solution.py:26
  70.7 1.5 collective-permute-start.12
  72.2 10.3 %collective-permute-done.9.refs_3_ = bf16[1024,256]{1,0:T(8,128)(2,1)} collective-permute-done((bf16[1024,256]{1,0:T(8,128)(2,1)}, bf16[1024,256]{1,0:T(8,128)(2,1)}, u32[]{:S(2)}, u32[]{:S(2)}) %collective-permute-start.9) | collective-permute-done | bytes 524320 | tf_op jit(solution)/shard_map/ppermute | solution.py:26
  82.5 1.5 collective-permute-start.4
  84.2 1.9 copy-done.4
  86.1 1.9 copy-done.7
  88.0 4.9 %hidden.3.hidden_ref = bf16[1024,768]{1,0:T(8,128)(2,1)S(1)} custom-call(s32[2]{0:T(128)S(1)} %pad_add_fusion.2.at_ref, bf16[768,2048]{1,0:T(8,128)(2,1)S(1)} %copy-done.4, bf16[768,2048]{1,0:T(8,128)(2,1)S(1)} %copy-done.7, f32[3,2048]{1,0:T(4,128)S(1)} %copy-done.11, f32[3,2048]{1,0:T(4,128)S(1)} %copy-done.12, f32[1,2048]{1,0:T(1,128)S(1)} %bitcast.60, ...), custom_call_target="tpu_custom_call" | custom-call | flops 2359296000 | bytes 4718592 | tf_op jit(solution)/shard_map/hidden/pallas_call | solution.py:92
  93.5 5.7 %own.1.before_ref = f32[8,1024,256]{2,1,0:T(8,128)S(1)} custom-call(s32[8]{0:T(128)S(1)} %stack.98.at_ref, bf16[1024,768]{1,0:T(8,128)(2,1)S(1)} %hidden.3.hidden_ref, bf16[768,2048]{1,0:T(8,128)(2,1)S(1)} %copy-done), custom_call_target="tpu_custom_call" | custom-call | flops 3221225472 | bytes 4718592 | tf_op jit(solution)/shard_map/own/pallas_call | solution.py:133
  99.2 3.3 %copy-done.1 = f32[8,1024,256]{2,1,0:T(8,128)} copy-done((f32[8,1024,256]{2,1,0:T(8,128)}, f32[8,1024,256]{2,1,0:T(8,128)S(1)}, u32[]{:S(2)}) %copy-start.1) | copy-done | bytes 8388632
  102.5 1.5 collective-permute-start.3
  104.1 2.7 %collective-permute-start.2 = (bf16[1024,256]{1,0:T(8,128)(2,1)}, bf16[1024,256]{1,0:T(8,128)(2,1)}, u32[]{:S(2)}, u32[]{:S(2)}) collective-permute-start(bf16[1024,256]{1,0:T(8,128)(2,1)} %collective-permute-done.refs_1_), channel_id=1, source_target_pairs={{0,4},{2,6},{4,8},{6,10},{8,12},{10,14},{12,0},{14,2},{1,5},{3,7},... | collective-permute-start | bytes 1572872 | tf_op jit(solution)/shard_map/ppermute | solution.py:26
  108.1 2.1 collective-permute-start.6
  110.3 3.4 %copy-done.2 = f32[8,1024,256]{2,1,0:T(8,128)S(1)} copy-done((f32[8,1024,256]{2,1,0:T(8,128)S(1)}, f32[8,1024,256]{2,1,0:T(8,128)}, u32[]{:S(2)}) %copy-start.2) | copy-done | bytes 8388632
  113.7 5.5 %outer.3 = (bf16[2,512,256]{2,1,0:T(8,128)(2,1)S(1)}, bf16[2,512,256]{2,1,0:T(8,128)(2,1)S(1)}, bf16[2,512,256]{2,1,0:T(8,128)(2,1)S(1)}, bf16[1,512,256]{2,1,0:T(8,128)(2,1)S(1)}, bf16[1,512,256]{2,1,0:T(8,128)(2,1)S(1)}) custom-call(s32[4]{0:T(128)S(1)} %pad_add_fusion.3.at_ref, bf16[1024,768]{1,0:T(8,128)(2,1)} %collective-permute-done.14.hidden_ref, ...), custom_call_target="tpu_custom_call" | custom-call | flops 1610612736 | bytes 3145728 | tf_op jit(solution)/shard_map/outer/pallas_call | solution.py:179
  120.3 8.6 %gate.4 = (bf16[768,2048]{1,0:T(8,128)(2,1)}, bf16[768,2048]{1,0:T(8,128)(2,1)}, f32[8,2048]{1,0:T(8,128)S(1)}) custom-call(s32[8]{0:T(128)S(1)} %stack.87.at_ref, bf16[768,2048]{1,0:T(8,128)(2,1)S(1)} %copy-done, bf16[2048,256]{1,0:T(8,128)(2,1)S(1)} %copy-done.10, bf16[1024,256]{1,0:T(8,128)(2,1)} %collective-permute-done.7.refs_1_, ...), custom_call_target="tpu_custom_call" | custom-call | flops 1966080000 | bytes 3145728 | tf_op jit(solution)/shard_map/gate/pallas_call | solution.py:286
  128.9 8.6 %gate.5 = (bf16[768,2048]{1,0:T(8,128)(2,1)}, bf16[768,2048]{1,0:T(8,128)(2,1)}, f32[8,2048]{1,0:T(8,128)S(1)}) custom-call(s32[8]{0:T(128)S(1)} %stack.87.at_ref, bf16[768,2048]{1,0:T(8,128)(2,1)S(1)} %copy-done, bf16[2048,256]{1,0:T(8,128)(2,1)S(1)} %copy-done.10, ...), custom_call_target="tpu_custom_call", output_to_operand_aliasing={{0}: (16, {}), {1}: (17, {}), {2}: (18, {})} | custom-call | flops 1966080000 | bytes 3145728 | tf_op jit(solution)/shard_map/gate/pallas_call | solution.py:286
  137.5 8.9 %gate.6 = (bf16[768,2048]{1,0:T(8,128)(2,1)}, bf16[768,2048]{1,0:T(8,128)(2,1)}, f32[8,2048]{1,0:T(8,128)S(1)}) custom-call(s32[8]{0:T(128)S(1)} %stack.87.at_ref, bf16[768,2048]{1,0:T(8,128)(2,1)S(1)} %copy-done, bf16[2048,256]{1,0:T(8,128)(2,1)S(1)} %copy-done.10, ...), custom_call_target="tpu_custom_call", output_to_operand_aliasing={{0}: (16, {}), {1}: (17, {}), {2}: (18, {})} | custom-call | flops 1966080000 | bytes 3145728 | tf_op jit(solution)/shard_map/gate/pallas_call | solution.py:286
  149.5 5.4 %outer.2 = (f32[2,512,256]{2,1,0:T(8,128)S(1)}, f32[2,512,256]{2,1,0:T(8,128)S(1)}, f32[2,512,256]{2,1,0:T(8,128)S(1)}, f32[1,512,256]{2,1,0:T(8,128)S(1)}, f32[1,512,256]{2,1,0:T(8,128)S(1)}) custom-call(s32[4]{0:T(128)S(1)} %pad_add_fusion.1.at_ref, bf16[1024,768]{1,0:T(8,128)(2,1)} %collective-permute-done.14.hidden_ref, f32[8,1024,256]{2,1,0:T(8,128)S(1)} %bitcast.58, ...), custom_call_target="tpu_custom_call" | custom-call | flops 1610612736 | bytes 3145728 | tf_op jit(solution)/shard_map/outer/pallas_call | solution.py:179
  155.1 3.2 %collective-permute-start.20 = (bf16[512,256]{1,0:T(8,128)(2,1)S(1)}, bf16[512,256]{1,0:T(8,128)(2,1)S(1)}, u32[]{:S(2)}, u32[]{:S(2)}) collective-permute-start(bf16[512,256]{1,0:T(8,128)(2,1)S(1)} %get-tuple-element.63), channel_id=1, source_target_pairs={{0,4},{2,6},{4,8},{6,10},{8,12},{10,14},{12,0},{14,2},{1,5},{3,7},... | collective-permute-start | bytes 786440 | tf_op jit(solution)/shard_map/ppermute | solution.py:26
  158.3 2.4 %collective-permute-start.19 = (bf16[512,256]{1,0:T(8,128)(2,1)S(1)}, bf16[512,256]{1,0:T(8,128)(2,1)S(1)}, u32[]{:S(2)}, u32[]{:S(2)}) collective-permute-start(bf16[512,256]{1,0:T(8,128)(2,1)S(1)} %get-tuple-element.62), channel_id=1, source_target_pairs={{0,12},{2,14},{4,0},{6,2},{8,4},{10,6},{12,8},{14,10},{1,13},{3,15... | collective-permute-start | bytes 786440 | tf_op jit(solution)/shard_map/ppermute | solution.py:26
  160.7 7.5 %collective-permute-done.23 = bf16[2,512,256]{2,1,0:T(8,128)(2,1)S(1)} collective-permute-done((bf16[2,512,256]{2,1,0:T(8,128)(2,1)S(1)}, bf16[2,512,256]{2,1,0:T(8,128)(2,1)S(1)}, u32[]{:S(2)}, u32[]{:S(2)}) %collective-permute-start.23) | collective-permute-done | bytes 524320 | tf_op jit(solution)/shard_map/ppermute | solution.py:20
  168.4 4.0 %collective-permute-start.26 = (bf16[512,256]{1,0:T(8,128)(2,1)S(1)}, bf16[512,256]{1,0:T(8,128)(2,1)S(1)}, u32[]{:S(2)}, u32[]{:S(2)}) collective-permute-start(bf16[512,256]{1,0:T(8,128)(2,1)S(1)} %get-tuple-element.65), channel_id=1, source_target_pairs={{0,4},{2,6},{4,8},{6,10},{8,12},{10,14},{12,0},{14,2},{1,5},{3,7},... | collective-permute-start | bytes 786440 | tf_op jit(solution)/shard_map/ppermute | solution.py:26
  173.9 8.6 %gate.7 = (bf16[768,2048]{1,0:T(8,128)(2,1)}, bf16[768,2048]{1,0:T(8,128)(2,1)}, f32[8,2048]{1,0:T(8,128)S(1)}) custom-call(s32[8]{0:T(128)S(1)} %stack.87.at_ref, bf16[768,2048]{1,0:T(8,128)(2,1)S(1)} %copy-done, bf16[2048,256]{1,0:T(8,128)(2,1)S(1)} %copy-done.10, ...), custom_call_target="tpu_custom_call", output_to_operand_aliasing={{0}: (16, {}), {1}: (17, {}), {2}: (18, {})} | custom-call | flops 1966080000 | bytes 3145728 | tf_op jit(solution)/shard_map/gate/pallas_call | solution.py:286
  183.8 2.7 %collective-permute-start.24 = (bf16[512,256]{1,0:T(8,128)(2,1)S(1)}, bf16[512,256]{1,0:T(8,128)(2,1)S(1)}, u32[]{:S(2)}, u32[]{:S(2)}) collective-permute-start(bf16[512,256]{1,0:T(8,128)(2,1)S(1)} %get-tuple-element.64), channel_id=1, source_target_pairs={{0,12},{2,14},{4,0},{6,2},{8,4},{10,6},{12,8},{14,10},{1,13},{3,15... | collective-permute-start | bytes 786440 | tf_op jit(solution)/shard_map/ppermute | solution.py:26
  186.9 2.0 collective-permute-done.22
  188.9 3.9 %collective-permute-done.24 = bf16[512,256]{1,0:T(8,128)(2,1)S(1)} collective-permute-done((bf16[512,256]{1,0:T(8,128)(2,1)S(1)}, bf16[512,256]{1,0:T(8,128)(2,1)S(1)}, u32[]{:S(2)}, u32[]{:S(2)}) %collective-permute-start.24) | collective-permute-done | bytes 262176 | tf_op jit(solution)/shard_map/ppermute | solution.py:26
  192.7 3.2 %collective-permute-done.27 = bf16[512,256]{1,0:T(8,128)(2,1)S(1)} collective-permute-done((bf16[512,256]{1,0:T(8,128)(2,1)S(1)}, bf16[512,256]{1,0:T(8,128)(2,1)S(1)}, u32[]{:S(2)}, u32[]{:S(2)}) %collective-permute-start.27) | collective-permute-done | bytes 262176 | tf_op jit(solution)/shard_map/ppermute | solution.py:26
  196.2 3.1 %collective-permute-start.28 = (f32[8,2176]{1,0:T(8,128)S(1)}, f32[8,2176]{1,0:T(8,128)S(1)}, u32[]{:S(2)}, u32[]{:S(2)}) collective-permute-start(f32[8,2176]{1,0:T(8,128)S(1)} %maximum_maximum_fusion), channel_id=1, source_target_pairs={{0,8},{2,10},{4,12},{6,14},{8,0},{10,2},{12,4},{14,6},{16,24},{18,... | collective-permute-start | bytes 208904 | tf_op jit(solution)/shard_map/ppermute | solution.py:20
  199.3 1.5 collective-permute-start.30
  201.6 2.0 collective-permute-done.29
  203.6 1.9 collective-permute-done.30
  207.6 1.5 collective-permute-start.33
  211.2 2.4 %collective-permute-done.33 = f32[8,2176]{1,0:T(8,128)S(1)} collective-permute-done((f32[8,2176]{1,0:T(8,128)S(1)}, f32[8,2176]{1,0:T(8,128)S(1)}, u32[]{:S(2)}, u32[]{:S(2)}) %collective-permute-start.33) | collective-permute-done | bytes 69664 | tf_op jit(solution)/shard_map/ppermute | solution.py:20
  215.5 4.7 %collective-permute-done.34 = f32[512,256]{1,0:T(8,128)S(1)} collective-permute-done((f32[512,256]{1,0:T(8,128)S(1)}, f32[512,256]{1,0:T(8,128)S(1)}, u32[]{:S(2)}, u32[]{:S(2)}) %collective-permute-start.34) | collective-permute-done | bytes 524320 | tf_op jit(solution)/shard_map/ppermute | solution.py:20
  220.3 5.5 %collective-permute-done.35 = f32[512,256]{1,0:T(8,128)S(1)} collective-permute-done((f32[512,256]{1,0:T(8,128)S(1)}, f32[512,256]{1,0:T(8,128)S(1)}, u32[]{:S(2)}, u32[]{:S(2)}) %collective-permute-start.35) | collective-permute-done | bytes 524320 | tf_op jit(solution)/shard_map/ppermute | solution.py:20
  (98 shorter events, 20.1 us)
Async XLA Ops:
  0.6 13.2 %copy-start.3 = (bf16[768,2048]{1,0:T(8,128)(2,1)S(1)}, bf16[768,2048]{1,0:T(8,128)(2,1)}, u32[]{:S(2)}) copy-start(bf16[768,2048]{1,0:T(8,128)(2,1)} %gate_ref.3) | copy-start | bytes 9437188
  0.7 13.2 %copy-start.11 = (f32[3,2048]{1,0:T(4,128)S(1)}, f32[3,2048]{1,0:T(4,128)}, u32[]{:S(2)}) copy-start(f32[3,2048]{1,0:T(4,128)} %tg_ref.3) | copy-start | bytes 73732
  0.7 13.2 %copy-start.12 = (f32[3,2048]{1,0:T(4,128)S(1)}, f32[3,2048]{1,0:T(4,128)}, u32[]{:S(2)}) copy-start(f32[3,2048]{1,0:T(4,128)} %tl_ref.3) | copy-start | bytes 73732
  0.7 13.2 %copy-start.13 = (f32[2048]{0:T(1024)S(1)}, f32[2048]{0:T(1024)}, u32[]{:S(2)}) copy-start(f32[2048]{0:T(1024)} %param.12) | copy-start | bytes 24580
  0.7 13.2 %copy-start.14 = (f32[2048]{0:T(1024)S(1)}, f32[2048]{0:T(1024)}, u32[]{:S(2)}) copy-start(f32[2048]{0:T(1024)} %param.13) | copy-start | bytes 24580
  3.6 38.5 %collective-permute-start.15 = (bf16[384,2048]{1,0:T(8,128)(2,1)}, bf16[384,2048]{1,0:T(8,128)(2,1)}, u32[]{:S(2)}, u32[]{:S(2)}) collective-permute-start(bf16[384,2048]{1,0:T(8,128)(2,1)} %constant_dynamic-slice_fusion), channel_id=1, source_target_pairs={{0,16},{16,0},{1,17},{17,1},{2,18},{18,2},{3,19},{19,3},{4,20},{20... | collective-permute-start | bytes 4718600 | tf_op jit(solution)/shard_map/ppermute | solution.py:20
  8.4 34.5 %collective-permute-start.7 = (bf16[1024,256]{1,0:T(8,128)(2,1)}, bf16[1024,256]{1,0:T(8,128)(2,1)}, u32[]{:S(2)}, u32[]{:S(2)}) collective-permute-start(bf16[1024,256]{1,0:T(8,128)(2,1)} %slice.53), channel_id=1, source_target_pairs={{0,4},{2,6},{4,8},{6,10},{8,12},{10,14},{12,0},{14,2},{1,5},{3,7},... | collective-permute-start | bytes 1572872 | tf_op jit(solution)/shard_map/ppermute | solution.py:26
  10.0 35.1 %collective-permute-start.8 = (bf16[1024,256]{1,0:T(8,128)(2,1)}, bf16[1024,256]{1,0:T(8,128)(2,1)}, u32[]{:S(2)}, u32[]{:S(2)}) collective-permute-start(bf16[1024,256]{1,0:T(8,128)(2,1)} %slice.53), channel_id=1, source_target_pairs={{0,12},{2,14},{4,0},{6,2},{8,4},{10,6},{12,8},{14,10},{1,13},{3,15... | collective-permute-start | bytes 1572872 | tf_op jit(solution)/shard_map/ppermute | solution.py:26
  12.2 34.9 %collective-permute-start.10 = (bf16[1024,256]{1,0:T(8,128)(2,1)}, bf16[1024,256]{1,0:T(8,128)(2,1)}, u32[]{:S(2)}, u32[]{:S(2)}) collective-permute-start(bf16[1024,256]{1,0:T(8,128)(2,1)} %slice.53), channel_id=1, source_target_pairs={{0,2},{2,0},{4,6},{6,4},{8,10},{10,8},{12,14},{14,12},{1,3},{3,1},... | collective-permute-start | bytes 1572872 | tf_op jit(solution)/shard_map/ppermute | solution.py:20
  15.7 26.4 %copy-start.9 = (bf16[2048,256]{1,0:T(8,128)(2,1)S(1)}, bf16[2048,256]{1,0:T(8,128)(2,1)}, u32[]{:S(2)}) copy-start(bf16[2048,256]{1,0:T(8,128)(2,1)} %refs_0_.7) | copy-start | bytes 3145732
  21.5 85.3 %collective-permute-start.14 = (bf16[1024,768]{1,0:T(8,128)(2,1)}, bf16[1024,768]{1,0:T(8,128)(2,1)}, u32[]{:S(2)}, u32[]{:S(2)}) collective-permute-start(bf16[1024,768]{1,0:T(8,128)(2,1)} %hidden.2), channel_id=1, source_target_pairs={{0,16},{16,0},{1,17},{17,1},{2,18},{18,2},{3,19},{19,3},{4,20},{20... | collective-permute-start | bytes 4718600 | tf_op jit(solution)/shard_map/ppermute | solution.py:20
  42.1 66.0 %collective-permute-start.16 = (bf16[384,2048]{1,0:T(8,128)(2,1)}, bf16[384,2048]{1,0:T(8,128)(2,1)}, u32[]{:S(2)}, u32[]{:S(2)}) collective-permute-start(bf16[384,2048]{1,0:T(8,128)(2,1)} %collective-permute-done.15.refs_0_), channel_id=1, source_target_pairs={{0,1},{1,0},{2,3},{3,2},{4,5},{5,4},{6,7},{7,6},{8,9},{9,8},{10,11... | collective-permute-start | bytes 4718600 | tf_op jit(solution)/shard_map/ppermute | solution.py:20
  42.9 17.3 %collective-permute-start = (bf16[1024,256]{1,0:T(8,128)(2,1)}, bf16[1024,256]{1,0:T(8,128)(2,1)}, u32[]{:S(2)}, u32[]{:S(2)}) collective-permute-start(bf16[1024,256]{1,0:T(8,128)(2,1)} %slice.52), channel_id=1, source_target_pairs={{0,4},{2,6},{4,8},{6,10},{8,12},{10,14},{12,0},{14,2},{1,5},{3,7},... | collective-permute-start | bytes 1572872 | tf_op jit(solution)/shard_map/ppermute | solution.py:26
  45.1 25.6 %collective-permute-start.1 = (bf16[1024,256]{1,0:T(8,128)(2,1)}, bf16[1024,256]{1,0:T(8,128)(2,1)}, u32[]{:S(2)}, u32[]{:S(2)}) collective-permute-start(bf16[1024,256]{1,0:T(8,128)(2,1)} %slice.52), channel_id=1, source_target_pairs={{0,12},{2,14},{4,0},{6,2},{8,4},{10,6},{12,8},{14,10},{1,13},{3,15... | collective-permute-start | bytes 1572872 | tf_op jit(solution)/shard_map/ppermute | solution.py:26
  47.1 35.4 %collective-permute-start.9 = (bf16[1024,256]{1,0:T(8,128)(2,1)}, bf16[1024,256]{1,0:T(8,128)(2,1)}, u32[]{:S(2)}, u32[]{:S(2)}) collective-permute-start(bf16[1024,256]{1,0:T(8,128)(2,1)} %collective-permute-done.7.refs_1_), channel_id=1, source_target_pairs={{0,4},{2,6},{4,8},{6,10},{8,12},{10,14},{12,0},{14,2},{1,5},{3,7},... | collective-permute-start | bytes 1572872 | tf_op jit(solution)/shard_map/ppermute | solution.py:26
  60.2 32.7 %collective-permute-start.11 = (bf16[1024,256]{1,0:T(8,128)(2,1)}, bf16[1024,256]{1,0:T(8,128)(2,1)}, u32[]{:S(2)}, u32[]{:S(2)}) collective-permute-start(bf16[1024,256]{1,0:T(8,128)(2,1)} %collective-permute-done.7.refs_1_), channel_id=1, source_target_pairs={{0,2},{2,0},{4,6},{6,4},{8,10},{10,8},{12,14},{14,12},{1,3},{3,1},... | collective-permute-start | bytes 1572872 | tf_op jit(solution)/shard_map/ppermute | solution.py:20
  70.7 31.9 %collective-permute-start.12 = (bf16[1024,256]{1,0:T(8,128)(2,1)}, bf16[1024,256]{1,0:T(8,128)(2,1)}, u32[]{:S(2)}, u32[]{:S(2)}) collective-permute-start(bf16[1024,256]{1,0:T(8,128)(2,1)} %collective-permute-done.8.refs_2_), channel_id=1, source_target_pairs={{0,2},{2,0},{4,6},{6,4},{8,10},{10,8},{12,14},{14,12},{1,3},{3,1},... | collective-permute-start | bytes 1572872 | tf_op jit(solution)/shard_map/ppermute | solution.py:20
  82.5 21.6 %collective-permute-start.4 = (bf16[1024,256]{1,0:T(8,128)(2,1)}, bf16[1024,256]{1,0:T(8,128)(2,1)}, u32[]{:S(2)}, u32[]{:S(2)}) collective-permute-start(bf16[1024,256]{1,0:T(8,128)(2,1)} %collective-permute-done.refs_1_), channel_id=1, source_target_pairs={{0,2},{2,0},{4,6},{6,4},{8,10},{10,8},{12,14},{14,12},{1,3},{3,1},... | collective-permute-start | bytes 1572872 | tf_op jit(solution)/shard_map/ppermute | solution.py:20
  88.0 5.5 %copy-start = (bf16[768,2048]{1,0:T(8,128)(2,1)S(1)}, bf16[768,2048]{1,0:T(8,128)(2,1)}, u32[]{:S(2)}) copy-start(bf16[768,2048]{1,0:T(8,128)(2,1)} %tokens_ref.9) | copy-start | bytes 9437188
  92.9 26.4 %collective-permute-start.13 = (bf16[1024,256]{1,0:T(8,128)(2,1)}, bf16[1024,256]{1,0:T(8,128)(2,1)}, u32[]{:S(2)}, u32[]{:S(2)}) collective-permute-start(bf16[1024,256]{1,0:T(8,128)(2,1)} %collective-permute-done.9.refs_3_), channel_id=1, source_target_pairs={{0,2},{2,0},{4,6},{6,4},{8,10},{10,8},{12,14},{14,12},{1,3},{3,1},... | collective-permute-start | bytes 1572872 | tf_op jit(solution)/shard_map/ppermute | solution.py:20
  102.5 34.9 %collective-permute-start.3 = (bf16[1024,256]{1,0:T(8,128)(2,1)}, bf16[1024,256]{1,0:T(8,128)(2,1)}, u32[]{:S(2)}, u32[]{:S(2)}) collective-permute-start(bf16[1024,256]{1,0:T(8,128)(2,1)} %slice.52), channel_id=1, source_target_pairs={{0,2},{2,0},{4,6},{6,4},{8,10},{10,8},{12,14},{14,12},{1,3},{3,1},... | collective-permute-start | bytes 1572872 | tf_op jit(solution)/shard_map/ppermute | solution.py:20
  104.1 33.4 %collective-permute-start.2 = (bf16[1024,256]{1,0:T(8,128)(2,1)}, bf16[1024,256]{1,0:T(8,128)(2,1)}, u32[]{:S(2)}, u32[]{:S(2)}) collective-permute-start(bf16[1024,256]{1,0:T(8,128)(2,1)} %collective-permute-done.refs_1_), channel_id=1, source_target_pairs={{0,4},{2,6},{4,8},{6,10},{8,12},{10,14},{12,0},{14,2},{1,5},{3,7},... | collective-permute-start | bytes 1572872 | tf_op jit(solution)/shard_map/ppermute | solution.py:26
  106.8 30.7 %collective-permute-start.5 = (bf16[1024,256]{1,0:T(8,128)(2,1)}, bf16[1024,256]{1,0:T(8,128)(2,1)}, u32[]{:S(2)}, u32[]{:S(2)}) collective-permute-start(bf16[1024,256]{1,0:T(8,128)(2,1)} %collective-permute-done.1.refs_2_), channel_id=1, source_target_pairs={{0,2},{2,0},{4,6},{6,4},{8,10},{10,8},{12,14},{14,12},{1,3},{3,1},... | collective-permute-start | bytes 1572872 | tf_op jit(solution)/shard_map/ppermute | solution.py:20
  108.1 29.4 %collective-permute-start.6 = (bf16[1024,256]{1,0:T(8,128)(2,1)}, bf16[1024,256]{1,0:T(8,128)(2,1)}, u32[]{:S(2)}, u32[]{:S(2)}) collective-permute-start(bf16[1024,256]{1,0:T(8,128)(2,1)} %collective-permute-done.4.refs_5_), channel_id=1, source_target_pairs={{0,4},{2,6},{4,8},{6,10},{8,12},{10,14},{12,0},{14,2},{1,5},{3,7},... | collective-permute-start | bytes 1572872 | tf_op jit(solution)/shard_map/ppermute | solution.py:26
  113.7 6.6 %copy-start.5 = (bf16[768,2048]{1,0:T(8,128)(2,1)S(1)}, bf16[768,2048]{1,0:T(8,128)(2,1)}, u32[]{:S(2)}) copy-start(bf16[768,2048]{1,0:T(8,128)(2,1)} %gate_ref.3) | copy-start | bytes 9437188
  113.7 6.6 %copy-start.8 = (bf16[768,2048]{1,0:T(8,128)(2,1)S(1)}, bf16[768,2048]{1,0:T(8,128)(2,1)}, u32[]{:S(2)}) copy-start(bf16[768,2048]{1,0:T(8,128)(2,1)} %linear_ref.3) | copy-start | bytes 9437188
  113.7 6.6 %copy-start.10 = (bf16[2048,256]{1,0:T(8,128)(2,1)S(1)}, bf16[2048,256]{1,0:T(8,128)(2,1)}, u32[]{:S(2)}) copy-start(bf16[2048,256]{1,0:T(8,128)(2,1)} %refs_0_.7) | copy-start | bytes 3145732
  119.3 35.6 %collective-permute-start.18 = (bf16[2,512,256]{2,1,0:T(8,128)(2,1)S(1)}, bf16[2,512,256]{2,1,0:T(8,128)(2,1)S(1)}, u32[]{:S(2)}, u32[]{:S(2)}) collective-permute-start(bf16[2,512,256]{2,1,0:T(8,128)(2,1)S(1)} %get-tuple-element.47), channel_id=1, source_target_pairs={{0,2},{2,0},{4,6},{6,4},{8,10},{10,8},{12,14},{14,12},{1,3},{3,1},... | collective-permute-start | bytes 1572872 | tf_op jit(solution)/shard_map/ppermute | solution.py:20
  137.5 12.0 %slice-start = ((s8[8388608]{0:T(1024)(128)(4,1)}), s8[4194304]{0:T(1024)(128)(4,1)S(1)}, s32[]{:S(2)}) async-start(s8[8388608]{0:T(1024)(128)(4,1)} %bitcast.57), calls=%async_computation | async-start | bytes 8388608
  137.5 12.0 %slice-start.1 = ((s8[8388608]{0:T(1024)(128)(4,1)}), s8[4194304]{0:T(1024)(128)(4,1)S(1)}, s32[]{:S(2)}) async-start(s8[8388608]{0:T(1024)(128)(4,1)} %bitcast.57), calls=%async_computation.1 | async-start | bytes 8388608
  146.4 26.0 %collective-permute-start.17 = (bf16[2,512,256]{2,1,0:T(8,128)(2,1)S(1)}, bf16[2,512,256]{2,1,0:T(8,128)(2,1)S(1)}, u32[]{:S(2)}, u32[]{:S(2)}) collective-permute-start(bf16[2,512,256]{2,1,0:T(8,128)(2,1)S(1)} %get-tuple-element.45), channel_id=1, source_target_pairs={{0,2},{2,0},{4,6},{6,4},{8,10},{10,8},{12,14},{14,12},{1,3},{3,1},... | collective-permute-start | bytes 1572872 | tf_op jit(solution)/shard_map/ppermute | solution.py:20
  147.5 20.7 %collective-permute-start.23 = (bf16[2,512,256]{2,1,0:T(8,128)(2,1)S(1)}, bf16[2,512,256]{2,1,0:T(8,128)(2,1)S(1)}, u32[]{:S(2)}, u32[]{:S(2)}) collective-permute-start(bf16[2,512,256]{2,1,0:T(8,128)(2,1)S(1)} %get-tuple-element.51), channel_id=1, source_target_pairs={{0,2},{2,0},{4,6},{6,4},{8,10},{10,8},{12,14},{14,12},{1,3},{3,1},... | collective-permute-start | bytes 1572872 | tf_op jit(solution)/shard_map/ppermute | solution.py:20
  148.4 35.4 %collective-permute-start.25 = (bf16[1,512,256]{2,1,0:T(8,128)(2,1)S(1)}, bf16[1,512,256]{2,1,0:T(8,128)(2,1)S(1)}, u32[]{:S(2)}, u32[]{:S(2)}) collective-permute-start(bf16[1,512,256]{2,1,0:T(8,128)(2,1)S(1)} %get-tuple-element.53), channel_id=1, source_target_pairs={{0,2},{2,0},{4,6},{6,4},{8,10},{10,8},{12,14},{14,12},{1,3},{3,1},... | collective-permute-start | bytes 786440 | tf_op jit(solution)/shard_map/ppermute | solution.py:20
  155.1 17.4 %collective-permute-start.20 = (bf16[512,256]{1,0:T(8,128)(2,1)S(1)}, bf16[512,256]{1,0:T(8,128)(2,1)S(1)}, u32[]{:S(2)}, u32[]{:S(2)}) collective-permute-start(bf16[512,256]{1,0:T(8,128)(2,1)S(1)} %get-tuple-element.63), channel_id=1, source_target_pairs={{0,4},{2,6},{4,8},{6,10},{8,12},{10,14},{12,0},{14,2},{1,5},{3,7},... | collective-permute-start | bytes 786440 | tf_op jit(solution)/shard_map/ppermute | solution.py:26
  158.3 28.4 %collective-permute-start.19 = (bf16[512,256]{1,0:T(8,128)(2,1)S(1)}, bf16[512,256]{1,0:T(8,128)(2,1)S(1)}, u32[]{:S(2)}, u32[]{:S(2)}) collective-permute-start(bf16[512,256]{1,0:T(8,128)(2,1)S(1)} %get-tuple-element.62), channel_id=1, source_target_pairs={{0,12},{2,14},{4,0},{6,2},{8,4},{10,6},{12,8},{14,10},{1,13},{3,15... | collective-permute-start | bytes 786440 | tf_op jit(solution)/shard_map/ppermute | solution.py:26
  168.4 18.2 %collective-permute-start.26 = (bf16[512,256]{1,0:T(8,128)(2,1)S(1)}, bf16[512,256]{1,0:T(8,128)(2,1)S(1)}, u32[]{:S(2)}, u32[]{:S(2)}) collective-permute-start(bf16[512,256]{1,0:T(8,128)(2,1)S(1)} %get-tuple-element.65), channel_id=1, source_target_pairs={{0,4},{2,6},{4,8},{6,10},{8,12},{10,14},{12,0},{14,2},{1,5},{3,7},... | collective-permute-start | bytes 786440 | tf_op jit(solution)/shard_map/ppermute | solution.py:26
  172.6 14.1 %collective-permute-start.21 = (bf16[512,256]{1,0:T(8,128)(2,1)S(1)}, bf16[512,256]{1,0:T(8,128)(2,1)S(1)}, u32[]{:S(2)}, u32[]{:S(2)}) collective-permute-start(bf16[512,256]{1,0:T(8,128)(2,1)S(1)} %fusion.1), channel_id=1, source_target_pairs={{0,4},{2,6},{4,8},{6,10},{8,12},{10,14},{12,0},{14,2},{1,5},{3,7},... | collective-permute-start | bytes 786440 | tf_op jit(solution)/shard_map/ppermute | solution.py:26
  182.5 6.4 %collective-permute-start.22 = (bf16[1,512,256]{2,1,0:T(8,128)(2,1)S(1)}, bf16[1,512,256]{2,1,0:T(8,128)(2,1)S(1)}, u32[]{:S(2)}, u32[]{:S(2)}) collective-permute-start(bf16[1,512,256]{2,1,0:T(8,128)(2,1)S(1)} %get-tuple-element.49), channel_id=1, source_target_pairs={{0,2},{2,0},{4,6},{6,4},{8,10},{10,8},{12,14},{14,12},{1,3},{3,1},... | collective-permute-start | bytes 786440 | tf_op jit(solution)/shard_map/ppermute | solution.py:20
  183.8 8.9 %collective-permute-start.24 = (bf16[512,256]{1,0:T(8,128)(2,1)S(1)}, bf16[512,256]{1,0:T(8,128)(2,1)S(1)}, u32[]{:S(2)}, u32[]{:S(2)}) collective-permute-start(bf16[512,256]{1,0:T(8,128)(2,1)S(1)} %get-tuple-element.64), channel_id=1, source_target_pairs={{0,12},{2,14},{4,0},{6,2},{8,4},{10,6},{12,8},{14,10},{1,13},{3,15... | collective-permute-start | bytes 786440 | tf_op jit(solution)/shard_map/ppermute | solution.py:26
  186.6 9.3 %collective-permute-start.27 = (bf16[512,256]{1,0:T(8,128)(2,1)S(1)}, bf16[512,256]{1,0:T(8,128)(2,1)S(1)}, u32[]{:S(2)}, u32[]{:S(2)}) collective-permute-start(bf16[512,256]{1,0:T(8,128)(2,1)S(1)} %fusion.4), channel_id=1, source_target_pairs={{0,4},{2,6},{4,8},{6,10},{8,12},{10,14},{12,0},{14,2},{1,5},{3,7},... | collective-permute-start | bytes 786440 | tf_op jit(solution)/shard_map/ppermute | solution.py:26
  196.2 5.4 %collective-permute-start.28 = (f32[8,2176]{1,0:T(8,128)S(1)}, f32[8,2176]{1,0:T(8,128)S(1)}, u32[]{:S(2)}, u32[]{:S(2)}) collective-permute-start(f32[8,2176]{1,0:T(8,128)S(1)} %maximum_maximum_fusion), channel_id=1, source_target_pairs={{0,8},{2,10},{4,12},{6,14},{8,0},{10,2},{12,4},{14,6},{16,24},{18,... | collective-permute-start | bytes 208904 | tf_op jit(solution)/shard_map/ppermute | solution.py:20
  199.3 4.3 %collective-permute-start.29 = (f32[8,2176]{1,0:T(8,128)S(1)}, f32[8,2176]{1,0:T(8,128)S(1)}, u32[]{:S(2)}, u32[]{:S(2)}) collective-permute-start(f32[8,2176]{1,0:T(8,128)S(1)} %maximum_maximum_fusion), channel_id=1, source_target_pairs={{0,4},{2,6},{4,0},{6,2},{8,12},{10,14},{12,8},{14,10},{16,20},{18,... | collective-permute-start | bytes 208904 | tf_op jit(solution)/shard_map/ppermute | solution.py:20
  199.3 6.2 %collective-permute-start.30 = (f32[8,2176]{1,0:T(8,128)S(1)}, f32[8,2176]{1,0:T(8,128)S(1)}, u32[]{:S(2)}, u32[]{:S(2)}) collective-permute-start(f32[8,2176]{1,0:T(8,128)S(1)} %maximum_maximum_fusion), channel_id=1, source_target_pairs={{0,12},{2,14},{4,8},{6,10},{8,4},{10,6},{12,0},{14,2},{16,28},{18,... | collective-permute-start | bytes 208904 | tf_op jit(solution)/shard_map/ppermute | solution.py:20
  205.6 5.6 %collective-permute-start.31 = (f32[8,2176]{1,0:T(8,128)S(1)}, f32[8,2176]{1,0:T(8,128)S(1)}, u32[]{:S(2)}, u32[]{:S(2)}) collective-permute-start(f32[8,2176]{1,0:T(8,128)S(1)} %add_add_fusion), channel_id=1, source_target_pairs={{0,2},{2,0},{4,6},{6,4},{8,10},{10,8},{12,14},{14,12},{16,18},{18,... | collective-permute-start | bytes 208904 | tf_op jit(solution)/shard_map/ppermute | solution.py:20
  206.1 5.1 %collective-permute-start.32 = (f32[8,2176]{1,0:T(8,128)S(1)}, f32[8,2176]{1,0:T(8,128)S(1)}, u32[]{:S(2)}, u32[]{:S(2)}) collective-permute-start(f32[8,2176]{1,0:T(8,128)S(1)} %add_add_fusion), channel_id=1, source_target_pairs={{0,16},{2,18},{4,20},{6,22},{8,24},{10,26},{12,28},{14,30},{16,0},... | collective-permute-start | bytes 208904 | tf_op jit(solution)/shard_map/ppermute | solution.py:20
  207.6 6.0 %collective-permute-start.33 = (f32[8,2176]{1,0:T(8,128)S(1)}, f32[8,2176]{1,0:T(8,128)S(1)}, u32[]{:S(2)}, u32[]{:S(2)}) collective-permute-start(f32[8,2176]{1,0:T(8,128)S(1)} %add_add_fusion), channel_id=1, source_target_pairs={{0,18},{2,16},{4,22},{6,20},{8,26},{10,24},{12,30},{14,28},{16,2},... | collective-permute-start | bytes 208904 | tf_op jit(solution)/shard_map/ppermute | solution.py:20
  209.1 11.1 %collective-permute-start.34 = (f32[512,256]{1,0:T(8,128)S(1)}, f32[512,256]{1,0:T(8,128)S(1)}, u32[]{:S(2)}, u32[]{:S(2)}) collective-permute-start(f32[512,256]{1,0:T(8,128)S(1)} %get-tuple-element.55), channel_id=1, source_target_pairs={{0,16},{16,0},{1,17},{17,1},{2,18},{18,2},{3,19},{19,3},{4,20},{20... | collective-permute-start | bytes 1572872 | tf_op jit(solution)/shard_map/ppermute | solution.py:20
  210.6 15.2 %collective-permute-start.35 = (f32[512,256]{1,0:T(8,128)S(1)}, f32[512,256]{1,0:T(8,128)S(1)}, u32[]{:S(2)}, u32[]{:S(2)}) collective-permute-start(f32[512,256]{1,0:T(8,128)S(1)} %get-tuple-element.57), channel_id=1, source_target_pairs={{0,16},{16,0},{1,17},{17,1},{2,18},{18,2},{3,19},{19,3},{4,20},{20... | collective-permute-start | bytes 1572872 | tf_op jit(solution)/shard_map/ppermute | solution.py:20
  (5 other events, 12.4 us)
